TPU v7x, 32 devices: a whole 2x2x4 slice. The times are simulated.
32 devices in a mesh: sp: 8 (over z, x), dp: 4 (over y, core).
Axes of the slice: x: 2, y: 2, z: 4, core: 2. Of those that a mesh axis runs over, the one named last changes fastest.
Arguments:
- normed_input: bfloat16 [2560, 2048], P('sp'), may hold values from -6 to 6
- out_grad: bfloat16 [2560, 2048], P('sp'), may hold values from -6 to 6
- value_weight: bfloat16 [2048, 1024], P(None, 'dp'), may hold values from -0.125 to 0.125
- gate_weight: bfloat16 [2048, 1024], P(None, 'dp'), may hold values from -0.125 to 0.125
- down_weight: bfloat16 [1024, 2048], P('dp'), may hold values from -0.1875 to 0.1875
- conv_kernel: float32 [31, 1024], P(None, 'dp'), may hold values from -5 to 5
- conv_bias: float32 [1024], P('dp'), may hold values from -3 to 3
- norm_gain: float32 [1024], P('dp'), may hold values from 0.1 to 1.9
- norm_shift: float32 [1024], P('dp'), may hold values from -3 to 3
Outputs:
- input_grad: bfloat16 [2560, 2048], P('sp')
- value_grad: float32 [2048, 1024], P('sp', 'dp')
- gate_grad: float32 [2048, 1024], P('sp', 'dp')
- down_grad: float32 [1024, 2048], P('dp', 'sp')
- kernel_grad: float32 [31, 1024], P(None, 'dp')
- bias_grad: float32 [1024], P('dp')
- gain_grad: float32 [1024], P('dp')
- shift_grad: float32 [1024], P('dp')
All inputs are finite; a program needn't handle non-finite values.
Results may differ from a plain program's by a relative error of at most 0.006.
Values may be sent and summed in bfloat16 or wider, within the bound.
A program may use at most 64 MiB of HBM per device.

v0:
```python
import functools
import math

import jax
import jax.numpy as jnp
from jax import lax
from jax.experimental import pallas as pl
from jax.experimental.pallas import tpu as pltpu
from jax.sharding import PartitionSpec as P

EPS = 1e-05
F32 = jnp.float32
BF16 = jnp.bfloat16
MESH = pl.DeviceIdType.MESH
NT = (((1,), (1,)), ((), ()))
TN = (((0,), (0,)), ((), ()))
EXACT = lax.Precision.HIGHEST
PAD = 16
ROWS = 32
MAIN = 61_900_000
FINISH = 16_000_000


def dot(a, b, numbers, precision=None):
    return lax.dot_general(a, b, numbers, precision=precision, preferred_element_type=F32)


def kernel(
    sp,
    dp,
    ratio,
    x_hbm,
    og_hbm,
    wv_hbm,
    wg_hbm,
    wd_hbm,
    ck,
    bias,
    gain,
    shift,
    ig_out,
    vg_out,
    gg_out,
    dg_out,
    small_out,
    x,
    og,
    wv,
    wg,
    wd,
    load_sem,
    value,
    opening,
    glu,
    mixed,
    d_act,
    d_pad,
    act,
    dv,
    dg,
    cols,
    stats,
    stats2,
    part,
    ring_src,
    ring_dst,
    ig_send,
    ig_recv,
    ig_own,
    ig_sum,
    ig_peer,
    small,
    small_recv,
    halo_send,
    halo_recv,
    stat_send,
    stat_recv,
    ring_send,
    ring_recv,
    ig_ssem,
    ig_rsem,
    small_ssem,
    small_rsem,
):
    tokens, width = x.shape
    taps, chans = ck.shape
    channels = chans * dp
    reach = taps // 2
    chunk = width // sp
    half_chunk = chunk // 2
    tile = min(256, width)
    s = lax.axis_index("sp")
    d = lax.axis_index("dp")
    bits_sp = sp.bit_length() - 1
    bits_dp = dp.bit_length() - 1

    def flip(i, bit):
        step = 1 << bit
        return i + step * (1 - 2 * lax.rem(lax.div(i, step), 2))

    def index_of(p):
        far = lax.div(p, sp // 2)
        return (1 - far) * 2 * p + far * (2 * sp - 1 - 2 * p)

    odd = lax.rem(s, 2)
    pos = (1 - odd) * lax.div(s, 2) + odd * (sp - 1 - lax.div(s, 2))
    ahead = index_of(lax.rem(pos + 1, sp))
    behind = index_of(lax.rem(pos + sp - 1, sp))

    loads = [
        pltpu.make_async_copy(src, dst, load_sem.at[at])
        for at, (src, dst) in enumerate(
            [(x_hbm, x), (wv_hbm, wv), (wg_hbm, wg), (og_hbm, og), (wd_hbm, wd)]
        )
    ]
    for load in loads:
        load.start()

    barrier = pltpu.get_barrier_semaphore()
    peers = [ahead, behind, lax.rem(s + 1, sp), lax.rem(s + sp - 1, sp)]
    peers += [flip(s, bit) for bit in range(bits_sp)]
    for peer in peers:
        pl.semaphore_signal(barrier, inc=1, device_id={"sp": peer}, device_id_type=MESH)
    for off in range(1, dp):
        pl.semaphore_signal(
            barrier, inc=1, device_id={"dp": lax.rem(d + off, dp)}, device_id_type=MESH
        )

    numbers = (((1,), (0,)), ((), ()))
    loads[0].wait()
    loads[1].wait()
    value[...] = dot(x[...], wv[...], numbers).astype(BF16).astype(F32)
    loads[2].wait()
    opening[...] = dot(x[...], wg[...], numbers).astype(BF16).astype(F32)

    def row_loop(fn, init=None, rows=ROWS):
        def step(i, carry):
            return fn(pl.multiple_of(i * rows, rows), carry)

        return lax.fori_loop(0, tokens // rows, step, init)

    def make_glu(r, _):
        here = pl.ds(r, ROWS)
        o = jax.nn.sigmoid(opening[here, :])
        opening[here, :] = o
        glu[pl.ds(r + PAD, ROWS), :] = value[here, :] * o

    row_loop(make_glu)
    pl.semaphore_wait(barrier, len(peers) + dp - 1)

    has_low, has_high = s > 0, s < sp - 1

    def halo_copies(buf, at):
        up = pltpu.make_async_remote_copy(
            src_ref=buf.at[pl.ds(tokens, PAD)],
            dst_ref=buf.at[pl.ds(0, PAD)],
            send_sem=halo_send.at[at],
            recv_sem=halo_recv.at[at],
            device_id={"sp": lax.rem(s + 1, sp)},
            device_id_type=MESH,
        )
        down = pltpu.make_async_remote_copy(
            src_ref=buf.at[pl.ds(PAD, PAD)],
            dst_ref=buf.at[pl.ds(tokens + PAD, PAD)],
            send_sem=halo_send.at[at + 1],
            recv_sem=halo_recv.at[at + 1],
            device_id={"sp": lax.rem(s + sp - 1, sp)},
            device_id_type=MESH,
        )
        return up, down

    def halo_start(buf, at):
        up, down = halo_copies(buf, at)
        pl.when(has_high)(up.start)
        pl.when(has_low)(down.start)

        @pl.when(s == 0)
        def _():
            buf[pl.ds(0, PAD), :] = jnp.zeros((PAD, chans), F32)

        @pl.when(s == sp - 1)
        def _():
            buf[pl.ds(tokens + PAD, PAD), :] = jnp.zeros((PAD, chans), F32)

    def halo_wait(buf, at):
        up, down = halo_copies(buf, at)

        @pl.when(has_low)
        def _():
            up.wait_recv()
            down.wait_send()

        @pl.when(has_high)
        def _():
            down.wait_recv()
            up.wait_send()

    halo_start(glu, 0)
    loads[3].wait()
    loads[4].wait()
    d_act[...] = dot(og[...], wd[...], NT)
    halo_wait(glu, 0)

    span = ROWS + 2 * PAD

    def shifted(buf, r, offset):
        window = buf[pl.ds(r, span), :]
        return pltpu.roll(window, span - offset, 0) if offset else window

    def slide(buf, r, offset_of, acc):
        for low in range(8):
            those = [tap for tap in range(taps) if offset_of(tap) % 8 == low]
            if those:
                window = shifted(buf, r, low)
                for tap in those:
                    high = offset_of(tap) - low
                    acc = acc + ck[tap : tap + 1, :] * window[high : high + ROWS]
        return acc

    def conv(r, _):
        acc = jnp.zeros((ROWS, chans), F32) + bias[...]
        mixed[pl.ds(r, ROWS), :] = slide(glu, r, lambda tap: tap + PAD - reach, acc)

    row_loop(conv)

    ones = jnp.ones((8, chans), F32)
    line = lax.broadcasted_iota(jnp.int32, (8, tokens), 0)
    eye = (
        lax.broadcasted_iota(jnp.int32, (8, 128), 0)
        == lax.broadcasted_iota(jnp.int32, (8, 128), 1)
    ).astype(F32)

    def stat_copy(buf, off, at):
        return pltpu.make_async_remote_copy(
            src_ref=buf.at[0],
            dst_ref=buf.at[off],
            send_sem=stat_send.at[at * dp + off],
            recv_sem=stat_recv.at[at * dp + off],
            device_id={"dp": lax.rem(d + off, dp)},
            device_id_type=MESH,
        )

    def stat_start(buf, at, one, two):
        buf[0] = jnp.where(line == 0, dot(ones, one, NT, EXACT), dot(ones, two, NT, EXACT))
        for off in range(1, dp):
            stat_copy(buf, off, at).start()

    def stat_wait(buf, at):
        for off in range(1, dp):
            stat_copy(buf, off, at).wait()
        total = buf[0]
        for off in range(1, dp):
            total = total + buf[off]
        return total * (1.0 / channels)

    stat_start(stats, 0, mixed[...], mixed[...] * mixed[...])
    moments = stat_wait(stats, 0)
    mean = moments[0:1]
    inv = lax.rsqrt(moments[1:2] - mean * mean + EPS)
    cols[0] = dot(jnp.where(line == 0, mean, inv), eye, TN, EXACT)

    def norm(r, carry):
        gain_sum, shift_sum = carry
        here = pl.ds(r, ROWS)
        col = cols[0, here, :]
        centred = (mixed[here, :] - col[:, 0:1]) * col[:, 1:2]
        normed = centred * gain[...] + shift[...]
        sig = jax.nn.sigmoid(normed)
        act[here, :] = (normed * sig).astype(BF16)
        d_normed = d_act[here, :] * sig * (1.0 + normed * (1.0 - sig))
        mixed[here, :] = centred
        d_act[here, :] = d_normed * gain[...]
        gain_sum = gain_sum + jnp.sum(d_normed * centred, axis=0, keepdims=True)
        shift_sum = shift_sum + jnp.sum(d_normed, axis=0, keepdims=True)
        return gain_sum, shift_sum

    zero = jnp.zeros((1, chans), F32)
    gain_sum, shift_sum = row_loop(norm, (zero, zero))
    stat_start(stats2, 1, d_act[...], d_act[...] * mixed[...])

    def weight_grad(at, rows, factor):
        def step(i, _):
            here = pl.ds(pl.multiple_of(i * tile, tile), tile)
            part[at, here, :] = dot(rows[:, here], factor[...], TN) * ratio

        lax.fori_loop(0, width // tile, step, None)

    streams = [(0, 0, 1), (1, 0, -1), (0, 1, 1), (1, 1, -1), (2, 0, 1), (2, 1, -1)]
    late, early = (0, 1, 2, 3), (4, 5)

    def piece(stream, p):
        at, half, _ = streams[stream]
        first = index_of(lax.rem(p + 2 * sp, sp)) * chunk + half * half_chunk
        return part[at, pl.ds(pl.multiple_of(first, half_chunk), half_chunk), :]

    def ring_copy(stream, k):
        return pltpu.make_async_remote_copy(
            src_ref=ring_src.at[stream, k],
            dst_ref=ring_dst.at[stream, k],
            send_sem=ring_send.at[stream, k],
            recv_sem=ring_recv.at[stream, k],
            device_id={"sp": ahead if streams[stream][2] == 1 else behind},
            device_id_type=MESH,
        )

    def ring_step(k, which):
        for stream in which:
            way = streams[stream][2]
            mine = piece(stream, pos - way * (1 + k))
            if not (isinstance(k, int) and k == 0):
                ring_copy(stream, k - 1).wait_recv()
                mine = mine + ring_dst[stream, k - 1].astype(F32)
            ring_src[stream, k] = mine.astype(BF16)
            ring_copy(stream, k).start()

    def ring_end(which, outs):
        for stream in which:
            at, half, _ = streams[stream]
            ring_copy(stream, sp - 2).wait_recv()
            outs[at][pl.ds(half * half_chunk, half_chunk), :] = piece(stream, pos) + ring_dst[
                stream, sp - 2
            ].astype(F32)

    weight_grad(2, og, act)
    ring_step(0, early)

    moments = stat_wait(stats2, 1)
    cols[1] = dot(moments, eye, TN, EXACT)

    def norm_back(r, bias_sum):
        here = pl.ds(r, ROWS)
        col, back = cols[0, here, :], cols[1, here, :]
        d_mixed = col[:, 1:2] * (d_act[here, :] - back[:, 0:1] - mixed[here, :] * back[:, 1:2])
        d_pad[pl.ds(r + PAD, ROWS), :] = d_mixed
        return bias_sum + jnp.sum(d_mixed, axis=0, keepdims=True)

    bias_sum = row_loop(norm_back, zero)
    halo_start(d_pad, 2)

    small[0] = jnp.zeros(small.shape[1:], F32)
    for low in range(0, 8, 2):
        those = [
            [tap for tap in range(taps) if (tap + PAD - reach) % 8 == low + at] for at in range(2)
        ]

        def taps_sum(r, sums, low=low, those=those):
            grad = d_pad[pl.ds(r + PAD, ROWS), :]
            new = []
            for at in range(2):
                window = shifted(glu, r, low + at)
                for tap in those[at]:
                    high = tap + PAD - reach - low - at
                    prod = grad * window[high : high + ROWS]
                    acc = sums[len(new)]
                    for row in range(0, ROWS, 8):
                        acc = acc + prod[row : row + 8]
                    new.append(acc)
            return tuple(new)

        flat = those[0] + those[1]
        sums = row_loop(taps_sum, tuple(jnp.zeros((8, chans), F32) for _ in flat))
        for acc, tap in zip(sums, flat):
            small[0, tap : tap + 1, :] = jnp.sum(acc, axis=0, keepdims=True) * ratio
        if low == 2:
            ring_step(1, early)
    small[0, taps : taps + 1, :] = bias_sum * ratio
    small[0, taps + 1 : taps + 2, :] = gain_sum * ratio
    small[0, taps + 2 : taps + 3, :] = shift_sum * ratio

    def small_copy(bit):
        return pltpu.make_async_remote_copy(
            src_ref=small.at[bit],
            dst_ref=small_recv.at[bit],
            send_sem=small_ssem.at[bit],
            recv_sem=small_rsem.at[bit],
            device_id={"sp": flip(s, bit)},
            device_id_type=MESH,
        )

    def small_next(bit):
        small_copy(bit).wait_recv()
        return small[bit] + small_recv[bit]

    halo_wait(d_pad, 2)
    small_copy(0).start()

    def conv_back(r, _):
        here = pl.ds(r, ROWS)
        acc = jnp.zeros((ROWS, chans), F32)
        acc = slide(d_pad, r, lambda tap: PAD + reach - tap, acc)
        o = opening[here, :]
        grad = acc * o
        dv[here, :] = grad.astype(BF16)
        dg[here, :] = (grad * value[here, :] * (1.0 - o)).astype(BF16)

    row_loop(conv_back)
    weight_grad(0, x, dv)
    ring_step(0, late[0::2])
    weight_grad(1, x, dg)
    ring_step(0, late[1::2])
    ring_step(2, early)

    half = tokens // 2
    mine = pl.multiple_of(lax.rem(d, 2) * half, half)
    other = pl.multiple_of((1 - lax.rem(d, 2)) * half, half)

    def input_grad(first, target):
        def step(i, _):
            here = pl.ds(pl.multiple_of(i * tile, tile), tile)
            rows = pl.ds(first, half)
            got = dot(dv[rows, :], wv[here, :], NT) + dot(dg[rows, :], wg[here, :], NT)
            target[:, here] = got.astype(target.dtype)

        lax.fori_loop(0, width // tile, step, None)

    def ig_copy(at, src, dst, bit):
        return pltpu.make_async_remote_copy(
            src_ref=src,
            dst_ref=dst,
            send_sem=ig_ssem.at[at],
            recv_sem=ig_rsem.at[at],
            device_id={"dp": flip(d, bit)},
            device_id_type=MESH,
        )

    input_grad(other, ig_send)
    copy0 = ig_copy(0, ig_send, ig_recv, 0)
    copy0.start()
    input_grad(mine, ig_own)
    copy0.wait_recv()

    def wide_loop(fn):
        def step(i, _):
            fn(pl.ds(pl.multiple_of(i * tile, tile), tile))

        lax.fori_loop(0, width // tile, step, None)

    def pair_sum(here):
        ig_sum[0, :, here] = (ig_own[:, here] + ig_recv[:, here].astype(F32)).astype(BF16)

    def y_copy(bit):
        return ig_copy(bit, ig_sum.at[bit - 1], ig_peer.at[bit - 1], bit)

    wide_loop(pair_sum)
    last = bits_dp
    if last > 1:
        y_copy(1).start()
    small[1] = small_next(0)
    if bits_sp > 1:
        small_copy(1).start()

    everything = late + early
    ring_step(1, late)
    ring_step(3, early) if sp > 4 else None
    ring_step(2, late)
    for bit in range(1, bits_sp):
        small[bit + 1] = small_next(bit)
        if bit + 1 < bits_sp:
            small_copy(bit + 1).start()
    ring_step(3, late)

    for_early = 4

    def both(k, _):
        ring_step(k, everything)

    lax.fori_loop(for_early, sp - 2, both, None)

    for bit in range(1, bits_dp):
        y_copy(bit).wait_recv()

        def add(here, bit=bit):
            got = ig_sum[bit - 1, :, here].astype(F32) + ig_peer[bit - 1, :, here].astype(F32)
            ig_sum[bit, :, here] = got.astype(BF16)

        wide_loop(add)
        if bit + 1 < bits_dp:
            y_copy(bit + 1).start()

    final = bits_dp - 1
    give = ig_copy(
        bits_dp, ig_sum.at[final], ig_out.at[pl.ds(mine, half)], 0
    )
    give.start()
    ring_step(sp - 2, everything)

    def keep(here):
        ig_out[pl.ds(mine, half), here] = ig_sum[final, :, here]

    wide_loop(keep)
    small_out[...] = small[bits_sp]
    outs = (vg_out, gg_out, dg_out)
    ring_end(everything, outs)

    copy0.wait_send()
    for bit in range(1, bits_dp):
        y_copy(bit).wait_send()
    give.wait()
    for bit in range(bits_sp):
        small_copy(bit).wait_send()

    def drain(k, _):
        for stream in everything:
            ring_copy(stream, k).wait_send()

    lax.fori_loop(0, sp - 1, drain, None)


def finish(ig, vg, gg, dgrad, small, ig_o, vg_o, gg_o, dg_o, k_o, b_o, g_o, s_o, sem):
    copies = [
        pltpu.make_async_copy(src, dst, sem.at[at])
        for at, (src, dst) in enumerate([(ig, ig_o), (vg, vg_o), (gg, gg_o)])
    ]
    for copy in copies:
        copy.start()
    taps = k_o.shape[0]
    dg_o[...] = dgrad[...].T
    k_o[...] = small[0:taps, :]
    for at, out in enumerate((b_o, g_o, s_o)):
        out[...] = small[taps + at, :]
    for copy in copies:
        copy.wait()


def on_device(
    normed_input,
    out_grad,
    value_weight,
    gate_weight,
    down_weight,
    conv_kernel,
    conv_bias,
    norm_gain,
    norm_shift,
):
    tokens, width = normed_input.shape
    taps, chans = conv_kernel.shape
    sp, dp = lax.axis_size("sp"), lax.axis_size("dp")
    ratio = 1.0 / math.sqrt(tokens * sp)
    chunk = width // sp
    bits_sp, bits_dp = sp.bit_length() - 1, dp.bit_length() - 1
    small_rows = -(-(taps + 3) // 8) * 8
    half = tokens // 2
    full = (tokens, chans)
    vmem = pl.BlockSpec(memory_space=pltpu.VMEM)
    hbm = pl.BlockSpec(memory_space=pltpu.HBM)
    dma = pltpu.SemaphoreType.DMA
    ig, vg, gg, dgrad, small = pl.pallas_call(
        functools.partial(kernel, sp, dp, ratio),
        out_shape=(
            pltpu.VMEM((tokens, width), BF16),
            pltpu.VMEM((chunk, chans), F32),
            pltpu.VMEM((chunk, chans), F32),
            pltpu.VMEM((chunk, chans), F32),
            pltpu.VMEM((small_rows, chans), F32),
        ),
        in_specs=[hbm] * 5 + [vmem] * 4,
        out_specs=(vmem,) * 5,
        scratch_shapes=[
            pltpu.VMEM((tokens, width), BF16),
            pltpu.VMEM((tokens, width), BF16),
            pltpu.VMEM((width, chans), BF16),
            pltpu.VMEM((width, chans), BF16),
            pltpu.VMEM((chans, width), BF16),
            dma((5,)),
            pltpu.VMEM(full, F32),
            pltpu.VMEM(full, F32),
            pltpu.VMEM((tokens + 2 * PAD, chans), F32),
            pltpu.VMEM(full, F32),
            pltpu.VMEM(full, F32),
            pltpu.VMEM((tokens + 2 * PAD, chans), F32),
            pltpu.VMEM(full, BF16),
            pltpu.VMEM(full, BF16),
            pltpu.VMEM(full, BF16),
            pltpu.VMEM((2, tokens, 128), F32),
            pltpu.VMEM((dp, 8, tokens), F32),
            pltpu.VMEM((dp, 8, tokens), F32),
            pltpu.VMEM((3, width, chans), F32),
            pltpu.VMEM((6, sp - 1, chunk // 2, chans), BF16),
            pltpu.VMEM((6, sp - 1, chunk // 2, chans), BF16),
            pltpu.VMEM((half, width), BF16),
            pltpu.VMEM((half, width), BF16),
            pltpu.VMEM((half, width), F32),
            pltpu.VMEM((bits_dp, half, width), BF16),
            pltpu.VMEM((bits_dp - 1, half, width), BF16),
            pltpu.VMEM((bits_sp + 1, small_rows, chans), F32),
            pltpu.VMEM((bits_sp, small_rows, chans), F32),
            dma((4,)),
            dma((4,)),
            dma((2 * dp,)),
            dma((2 * dp,)),
            dma((6, sp - 1)),
            dma((6, sp - 1)),
            dma((bits_dp + 1,)),
            dma((bits_dp + 1,)),
            dma((bits_sp,)),
            dma((bits_sp,)),
        ],
        compiler_params=pltpu.CompilerParams(
            collective_id=0, has_side_effects=True, vmem_limit_bytes=MAIN
        ),
    )(
        normed_input,
        out_grad,
        value_weight,
        gate_weight,
        down_weight,
        conv_kernel,
        conv_bias[None, :],
        norm_gain[None, :],
        norm_shift[None, :],
    )
    row = jax.ShapeDtypeStruct((chans,), F32)
    return pl.pallas_call(
        finish,
        out_shape=(
            jax.ShapeDtypeStruct(ig.shape, BF16),
            jax.ShapeDtypeStruct(vg.shape, F32),
            jax.ShapeDtypeStruct(gg.shape, F32),
            jax.ShapeDtypeStruct((chans, chunk), F32),
            jax.ShapeDtypeStruct((taps, chans), F32),
            row,
            row,
            row,
        ),
        in_specs=[vmem] * 5,
        out_specs=(hbm,) * 3 + (vmem,) * 5,
        scratch_shapes=[dma((3,))],
        compiler_params=pltpu.CompilerParams(vmem_limit_bytes=FINISH),
    )(ig, vg, gg, dgrad, small)


def solution(mesh):
    in_specs = (
        P("sp", None),
        P("sp", None),
        P(None, "dp"),
        P(None, "dp"),
        P("dp", None),
        P(None, "dp"),
        P("dp"),
        P("dp"),
        P("dp"),
    )
    out_specs = (
        P("sp", None),
        P("sp", "dp"),
        P("sp", "dp"),
        P("dp", "sp"),
        P(None, "dp"),
        P("dp"),
        P("dp"),
        P("dp"),
    )
    return jax.shard_map(
        on_device, mesh=mesh, in_specs=in_specs, out_specs=out_specs, check_vma=False
    )
```

profile of v0, /device:TPU:0, one launch (start us, length us, event | category | flops | bytes accessed | tf_op | source)
XLA Modules:
  0.0 67.5 jit_solution(11890046101101131748)
XLA Ops:
  0.6 64.9 %shard_map.152 = (bf16[320,2048]{1,0:T(8,128)(2,1)S(1)}, f32[256,256]{1,0:T(8,128)S(1)}, f32[256,256]{1,0:T(8,128)S(1)}, f32[256,256]{1,0:T(8,128)S(1)}, f32[40,256]{1,0:T(8,128)S(1)}) custom-call(bf16[320,2048]{1,0:T(8,128)(2,1)} %x_hbm.1, bf16[320,2048]{1,0:T(8,128)(2,1)} %og_hbm.1, bf16[2048,256]{1,0:T(8,128)(2,1)} %wv_hbm.1, bf16[2048,256]{1,0:T(8,128)(2,1)} %wg_hbm.1, ...), custom_call_target="tpu_custom_call" | custom-call | tf_op jit(solution)/shard_map/pallas_call | solution.py:548
  65.5 2.0 %shard_map.153 = (bf16[320,2048]{1,0:T(8,128)(2,1)}, f32[256,256]{1,0:T(8,128)}, f32[256,256]{1,0:T(8,128)}, f32[256,256]{1,0:T(8,128)}, f32[31,256]{1,0:T(8,128...) custom-call(bf16[320,2048]{1,0:T(8,128)(2,1)S(1)} %get-tuple-element.13.ig, f32[256,256]{1,0:T(8,128)S(1)} %get-tuple-element.14.vg, ...), custom_call_target="tpu_custom_call" | custom-call | tf_op jit(solution)/shard_map/pallas_call | solution.py:614
where the time goes:
time: 67.7 us; the launch traced here: 67.5 us
  Pallas kernels  66.8 us (99%)
    pallas_call x1, Pallas kernels, on_device(): pl.pallas_call(functools.partial(kernel, sp, dp, ratio), out_shape=(pltpu...  64.9 us
    pallas_call x1, Pallas kernels, on_device(): pl.pallas_call(finish, out_shape=(jax.ShapeDtypeStruct(ig.shape, BF16), j...  1.98 us

commit v1 on v0

--- a/solution.py
+++ b/solution.py
@@ -12,17 +12,30 @@
 F32 = jnp.float32
 BF16 = jnp.bfloat16
 MESH = pl.DeviceIdType.MESH
+NN = (((1,), (0,)), ((), ()))
 NT = (((1,), (1,)), ((), ()))
 TN = (((0,), (0,)), ((), ()))
-EXACT = lax.Precision.HIGHEST
 PAD = 16
 ROWS = 32
+SUBS = 2
+GROUPS = 4
 MAIN = 61_900_000
 FINISH = 16_000_000
 
 
-def dot(a, b, numbers, precision=None):
-    return lax.dot_general(a, b, numbers, precision=precision, preferred_element_type=F32)
+def dot(a, b, numbers):
+    return lax.dot_general(a, b, numbers, preferred_element_type=F32)
+
+
+def split3(v):
+    high = v.astype(BF16)
+    rest = v - high.astype(F32)
+    mid = rest.astype(BF16)
+    return high, mid, (rest - mid.astype(F32)).astype(BF16)
+
+
+def is_wide(chunk, chans):
+    return chunk % 128 == 0 and chans % 32 == 0
 
 
 def kernel(
@@ -34,10 +47,10 @@
     wv_hbm,
     wg_hbm,
     wd_hbm,
-    ck,
-    bias,
-    gain,
-    shift,
+    ck_hbm,
+    bias_hbm,
+    gain_hbm,
+    shift_hbm,
     ig_out,
     vg_out,
     gg_out,
@@ -48,6 +61,10 @@
     wv,
     wg,
     wd,
+    ck,
+    bias,
+    gain,
+    shift,
     load_sem,
     value,
     opening,
@@ -58,6 +75,7 @@
     act,
     dv,
     dg,
+    turned,
     cols,
     stats,
     stats2,
@@ -87,7 +105,9 @@
     channels = chans * dp
     reach = taps // 2
     chunk = width // sp
-    half_chunk = chunk // 2
+    wide = is_wide(chunk, chans)
+    lines = chans if wide else chunk
+    strip = lines // (2 * SUBS)
     tile = min(256, width)
     s = lax.axis_index("sp")
     d = lax.axis_index("dp")
@@ -110,7 +130,17 @@
     loads = [
         pltpu.make_async_copy(src, dst, load_sem.at[at])
         for at, (src, dst) in enumerate(
-            [(x_hbm, x), (wv_hbm, wv), (wg_hbm, wg), (og_hbm, og), (wd_hbm, wd)]
+            [
+                (x_hbm, x),
+                (wv_hbm, wv),
+                (wg_hbm, wg),
+                (og_hbm, og),
+                (wd_hbm, wd),
+                (ck_hbm, ck),
+                (bias_hbm, bias),
+                (gain_hbm, gain),
+                (shift_hbm, shift),
+            ]
         )
     ]
     for load in loads:
@@ -126,18 +156,19 @@
             barrier, inc=1, device_id={"dp": lax.rem(d + off, dp)}, device_id_type=MESH
         )
 
-    numbers = (((1,), (0,)), ((), ()))
     loads[0].wait()
     loads[1].wait()
-    value[...] = dot(x[...], wv[...], numbers).astype(BF16).astype(F32)
+    value[...] = dot(x[...], wv[...], NN).astype(BF16).astype(F32)
     loads[2].wait()
-    opening[...] = dot(x[...], wg[...], numbers).astype(BF16).astype(F32)
+    opening[...] = dot(x[...], wg[...], NN).astype(BF16).astype(F32)
 
     def row_loop(fn, init=None, rows=ROWS):
         def step(i, carry):
             return fn(pl.multiple_of(i * rows, rows), carry)
 
         return lax.fori_loop(0, tokens // rows, step, init)
+
+    big = 80 if tokens % 80 == 0 else ROWS
 
     def make_glu(r, _):
         here = pl.ds(r, ROWS)
@@ -195,11 +226,23 @@
             down.wait_recv()
             up.wait_send()
 
+    def inner_outer(fn, between):
+        blocks = tokens // ROWS
+
+        def inner(i, _):
+            fn(pl.multiple_of(i * ROWS, ROWS), None)
+
+        def outer(i, _):
+            fn(pl.multiple_of(i * (blocks - 1) * ROWS, ROWS), None)
+
+        lax.fori_loop(1, blocks - 1, inner, None)
+        between()
+        lax.fori_loop(0, 2, outer, None)
+
     halo_start(glu, 0)
-    loads[3].wait()
-    loads[4].wait()
+    for load in loads[3:]:
+        load.wait()
     d_act[...] = dot(og[...], wd[...], NT)
-    halo_wait(glu, 0)
 
     span = ROWS + 2 * PAD
 
@@ -221,14 +264,24 @@
         acc = jnp.zeros((ROWS, chans), F32) + bias[...]
         mixed[pl.ds(r, ROWS), :] = slide(glu, r, lambda tap: tap + PAD - reach, acc)
 
-    row_loop(conv)
-
-    ones = jnp.ones((8, chans), F32)
+    inner_outer(conv, lambda: halo_wait(glu, 0))
+
+    ones = jnp.ones((16, chans), BF16)
     line = lax.broadcasted_iota(jnp.int32, (8, tokens), 0)
     eye = (
-        lax.broadcasted_iota(jnp.int32, (8, 128), 0)
-        == lax.broadcasted_iota(jnp.int32, (8, 128), 1)
-    ).astype(F32)
+        lax.rem(lax.broadcasted_iota(jnp.int32, (24, 128), 0), 8)
+        == lax.broadcasted_iota(jnp.int32, (24, 128), 1)
+    ).astype(BF16)
+    pieces = [(at, min(128, tokens - at)) for at in range(0, tokens, 128)]
+
+    def row_sums(v):
+        a, b, c = (dot(ones, term, NT) for term in split3(v))
+        return a + b + c
+
+    def columns(one, two):
+        both = jnp.where(line == 0, one, jnp.where(line == 1, two, 0.0))
+        terms = [term.astype(F32) for term in split3(both)]
+        return dot(jnp.concatenate(terms, axis=0).astype(BF16), eye, TN)
 
     def stat_copy(buf, off, at):
         return pltpu.make_async_remote_copy(
@@ -241,7 +294,10 @@
         )
 
     def stat_start(buf, at, one, two):
-        buf[0] = jnp.where(line == 0, dot(ones, one, NT, EXACT), dot(ones, two, NT, EXACT))
+        buf[0] = jnp.zeros(buf.shape[1:], F32)
+        for first, sums in ((0, row_sums(one)), (len(pieces), row_sums(two))):
+            for j, (begin, size) in enumerate(pieces):
+                buf[0, first + j : first + j + 1, 0:size] = sums[0:1, begin : begin + size]
         for off in range(1, dp):
             stat_copy(buf, off, at).start()
 
@@ -251,17 +307,23 @@
         total = buf[0]
         for off in range(1, dp):
             total = total + buf[off]
-        return total * (1.0 / channels)
+        total = total * (1.0 / channels)
+        one, two = (
+            jnp.concatenate(
+                [total[first + j : first + j + 1, 0:size] for j, (_, size) in enumerate(pieces)],
+                axis=1,
+            )
+            for first in (0, len(pieces))
+        )
+        return one, two
 
     stat_start(stats, 0, mixed[...], mixed[...] * mixed[...])
-    moments = stat_wait(stats, 0)
-    mean = moments[0:1]
-    inv = lax.rsqrt(moments[1:2] - mean * mean + EPS)
-    cols[0] = dot(jnp.where(line == 0, mean, inv), eye, TN, EXACT)
+    mean, square = stat_wait(stats, 0)
+    cols[0] = columns(mean, lax.rsqrt(square - mean * mean + EPS))
 
     def norm(r, carry):
         gain_sum, shift_sum = carry
-        here = pl.ds(r, ROWS)
+        here = pl.ds(r, big)
         col = cols[0, here, :]
         centred = (mixed[here, :] - col[:, 0:1]) * col[:, 1:2]
         normed = centred * gain[...] + shift[...]
@@ -275,23 +337,53 @@
         return gain_sum, shift_sum
 
     zero = jnp.zeros((1, chans), F32)
-    gain_sum, shift_sum = row_loop(norm, (zero, zero))
+    gain_sum, shift_sum = row_loop(norm, (zero, zero), big)
     stat_start(stats2, 1, d_act[...], d_act[...] * mixed[...])
 
-    def weight_grad(at, rows, factor):
+    def several(count, fn):
+        if count <= 8:
+            for i in range(count):
+                fn(i)
+        else:
+            lax.fori_loop(0, count, lambda i, _: fn(i), None)
+
+    def grad_tile(at, rows, off):
+        index = index_of(lax.rem(pos + off + 2 * sp, sp))
+        those = pl.ds(pl.multiple_of(index * chunk, chunk), chunk)
+        part[at, pl.ds(pl.multiple_of(index * lines, lines), lines), :] = dot(
+            turned[at], rows[:, those], NN
+        )
+
+    def grad_first(at, rows, factor):
+        if wide:
+            turned[at] = factor[...].T
+            grad_tile(at, rows, -1)
+            grad_tile(at, rows, 1)
+            return
+
         def step(i, _):
             here = pl.ds(pl.multiple_of(i * tile, tile), tile)
-            part[at, here, :] = dot(rows[:, here], factor[...], TN) * ratio
+            part[at, here, :] = dot(rows[:, here], factor[...], TN)
 
         lax.fori_loop(0, width // tile, step, None)
 
-    streams = [(0, 0, 1), (1, 0, -1), (0, 1, 1), (1, 1, -1), (2, 0, 1), (2, 1, -1)]
-    late, early = (0, 1, 2, 3), (4, 5)
+    def grad_rest(at, rows):
+        if wide:
+            several(sp - 2, lambda i: grad_tile(at, rows, (i + 2) % (sp - 1)))
+
+    streams = [
+        (at, 2 * sub + (way < 0), way) for at in range(3) for sub in range(SUBS) for way in (1, -1)
+    ]
+    early = [i for i, (at, _, _) in enumerate(streams) if at == 2]
+    late = [i for sub in range(SUBS) for i, (at, place, _) in enumerate(streams) if at < 2 and place // 2 == sub]
+
+    def late_of(at):
+        return [i for i in late if streams[i][0] == at]
 
     def piece(stream, p):
-        at, half, _ = streams[stream]
-        first = index_of(lax.rem(p + 2 * sp, sp)) * chunk + half * half_chunk
-        return part[at, pl.ds(pl.multiple_of(first, half_chunk), half_chunk), :]
+        at, place, _ = streams[stream]
+        first = index_of(lax.rem(p + 2 * sp, sp)) * lines + place * strip
+        return part[at, pl.ds(pl.multiple_of(first, strip), strip), :]
 
     def ring_copy(stream, k):
         return pltpu.make_async_remote_copy(
@@ -315,35 +407,112 @@
 
     def ring_end(which, outs):
         for stream in which:
-            at, half, _ = streams[stream]
+            at, place, _ = streams[stream]
             ring_copy(stream, sp - 2).wait_recv()
-            outs[at][pl.ds(half * half_chunk, half_chunk), :] = piece(stream, pos) + ring_dst[
-                stream, sp - 2
-            ].astype(F32)
-
-    weight_grad(2, og, act)
+            outs[at][pl.ds(place * strip, strip), :] = ratio * (
+                piece(stream, pos) + ring_dst[stream, sp - 2].astype(F32)
+            )
+
+    grad_first(2, og, act)
     ring_step(0, early)
-
-    moments = stat_wait(stats2, 1)
-    cols[1] = dot(moments, eye, TN, EXACT)
+    grad_rest(2, og)
+
+    first, second = stat_wait(stats2, 1)
+    cols[1] = columns(first, second)
 
     def norm_back(r, bias_sum):
-        here = pl.ds(r, ROWS)
+        here = pl.ds(r, big)
         col, back = cols[0, here, :], cols[1, here, :]
         d_mixed = col[:, 1:2] * (d_act[here, :] - back[:, 0:1] - mixed[here, :] * back[:, 1:2])
-        d_pad[pl.ds(r + PAD, ROWS), :] = d_mixed
+        d_pad[pl.ds(r + PAD, big), :] = d_mixed
         return bias_sum + jnp.sum(d_mixed, axis=0, keepdims=True)
 
-    bias_sum = row_loop(norm_back, zero)
+    bias_sum = row_loop(norm_back, zero, big)
     halo_start(d_pad, 2)
+    ring_step(1, early)
+
+    def conv_back(r, _):
+        here = pl.ds(r, ROWS)
+        acc = jnp.zeros((ROWS, chans), F32)
+        acc = slide(d_pad, r, lambda tap: PAD + reach - tap, acc)
+        o = opening[here, :]
+        grad = acc * o
+        dv[here, :] = grad.astype(BF16)
+        dg[here, :] = (grad * value[here, :] * (1.0 - o)).astype(BF16)
+
+    inner_outer(conv_back, lambda: halo_wait(d_pad, 2))
+    grad_first(0, x, dv)
+    ring_step(0, late_of(0))
+    grad_first(1, x, dg)
+    ring_step(0, late_of(1))
+    grad_rest(0, x)
+    grad_rest(1, x)
+    ring_step(2, early)
+
+    half = tokens // 2
+    mine = pl.multiple_of(lax.rem(d, 2) * half, half)
+    other = pl.multiple_of((1 - lax.rem(d, 2)) * half, half)
+    group = width // GROUPS
+
+    def ig_copy(at, g, src, dst, bit):
+        return pltpu.make_async_remote_copy(
+            src_ref=src,
+            dst_ref=dst,
+            send_sem=ig_ssem.at[at, g],
+            recv_sem=ig_rsem.at[at, g],
+            device_id={"dp": flip(d, bit)},
+            device_id_type=MESH,
+        )
+
+    def of_group(g):
+        return pl.ds(g * group, group)
+
+    def pair_copy(g):
+        return ig_copy(0, g, ig_send.at[:, of_group(g)], ig_recv.at[:, of_group(g)], 0)
+
+    def y_copy(bit, g):
+        return ig_copy(
+            bit, g, ig_sum.at[bit - 1, :, of_group(g)], ig_peer.at[bit - 1, :, of_group(g)], bit
+        )
+
+    final = bits_dp - 1
+
+    def give_copy(g):
+        return ig_copy(
+            bits_dp,
+            g,
+            ig_sum.at[final, :, of_group(g)],
+            ig_out.at[pl.ds(mine, half), of_group(g)],
+            0,
+        )
+
+    both_v = jnp.concatenate([dv[pl.ds(other, half), :], dv[pl.ds(mine, half), :]], axis=0)
+    both_g = jnp.concatenate([dg[pl.ds(other, half), :], dg[pl.ds(mine, half), :]], axis=0)
+    size = min(tile, group)
+    for g in range(GROUPS):
+        for begin in range(g * group, (g + 1) * group, size):
+            here = pl.ds(begin, size)
+            got = dot(both_v, wv[here, :], NT) + dot(both_g, wg[here, :], NT)
+            ig_send[:, here] = got[:half].astype(BF16)
+            ig_own[:, here] = got[half:]
+        pair_copy(g).start()
+
+    def pair_sums():
+        for g in range(GROUPS):
+            pair_copy(g).wait_recv()
+            here = of_group(g)
+            ig_sum[0, :, here] = (ig_own[:, here] + ig_recv[:, here].astype(F32)).astype(BF16)
+            if bits_dp > 1:
+                y_copy(1, g).start()
 
     small[0] = jnp.zeros(small.shape[1:], F32)
-    for low in range(0, 8, 2):
+
+    def taps_grad(low):
         those = [
             [tap for tap in range(taps) if (tap + PAD - reach) % 8 == low + at] for at in range(2)
         ]
 
-        def taps_sum(r, sums, low=low, those=those):
+        def taps_sum(r, sums):
             grad = d_pad[pl.ds(r + PAD, ROWS), :]
             new = []
             for at in range(2):
@@ -361,11 +530,6 @@
         sums = row_loop(taps_sum, tuple(jnp.zeros((8, chans), F32) for _ in flat))
         for acc, tap in zip(sums, flat):
             small[0, tap : tap + 1, :] = jnp.sum(acc, axis=0, keepdims=True) * ratio
-        if low == 2:
-            ring_step(1, early)
-    small[0, taps : taps + 1, :] = bias_sum * ratio
-    small[0, taps + 1 : taps + 2, :] = gain_sum * ratio
-    small[0, taps + 2 : taps + 3, :] = shift_sum * ratio
 
     def small_copy(bit):
         return pltpu.make_async_remote_copy(
@@ -377,147 +541,104 @@
             device_id_type=MESH,
         )
 
+    def small_first():
+        small[0, taps : taps + 1, :] = bias_sum * ratio
+        small[0, taps + 1 : taps + 2, :] = gain_sum * ratio
+        small[0, taps + 2 : taps + 3, :] = shift_sum * ratio
+        small_copy(0).start()
+
     def small_next(bit):
-        small_copy(bit).wait_recv()
-        return small[bit] + small_recv[bit]
-
-    halo_wait(d_pad, 2)
-    small_copy(0).start()
-
-    def conv_back(r, _):
-        here = pl.ds(r, ROWS)
-        acc = jnp.zeros((ROWS, chans), F32)
-        acc = slide(d_pad, r, lambda tap: PAD + reach - tap, acc)
-        o = opening[here, :]
-        grad = acc * o
-        dv[here, :] = grad.astype(BF16)
-        dg[here, :] = (grad * value[here, :] * (1.0 - o)).astype(BF16)
-
-    row_loop(conv_back)
-    weight_grad(0, x, dv)
-    ring_step(0, late[0::2])
-    weight_grad(1, x, dg)
-    ring_step(0, late[1::2])
-    ring_step(2, early)
-
-    half = tokens // 2
-    mine = pl.multiple_of(lax.rem(d, 2) * half, half)
-    other = pl.multiple_of((1 - lax.rem(d, 2)) * half, half)
-
-    def input_grad(first, target):
-        def step(i, _):
-            here = pl.ds(pl.multiple_of(i * tile, tile), tile)
-            rows = pl.ds(first, half)
-            got = dot(dv[rows, :], wv[here, :], NT) + dot(dg[rows, :], wg[here, :], NT)
-            target[:, here] = got.astype(target.dtype)
-
-        lax.fori_loop(0, width // tile, step, None)
-
-    def ig_copy(at, src, dst, bit):
-        return pltpu.make_async_remote_copy(
-            src_ref=src,
-            dst_ref=dst,
-            send_sem=ig_ssem.at[at],
-            recv_sem=ig_rsem.at[at],
-            device_id={"dp": flip(d, bit)},
-            device_id_type=MESH,
-        )
-
-    input_grad(other, ig_send)
-    copy0 = ig_copy(0, ig_send, ig_recv, 0)
-    copy0.start()
-    input_grad(mine, ig_own)
-    copy0.wait_recv()
-
-    def wide_loop(fn):
-        def step(i, _):
-            fn(pl.ds(pl.multiple_of(i * tile, tile), tile))
-
-        lax.fori_loop(0, width // tile, step, None)
-
-    def pair_sum(here):
-        ig_sum[0, :, here] = (ig_own[:, here] + ig_recv[:, here].astype(F32)).astype(BF16)
-
-    def y_copy(bit):
-        return ig_copy(bit, ig_sum.at[bit - 1], ig_peer.at[bit - 1], bit)
-
-    wide_loop(pair_sum)
-    last = bits_dp
-    if last > 1:
-        y_copy(1).start()
-    small[1] = small_next(0)
-    if bits_sp > 1:
-        small_copy(1).start()
-
-    everything = late + early
-    ring_step(1, late)
-    ring_step(3, early) if sp > 4 else None
-    ring_step(2, late)
-    for bit in range(1, bits_sp):
-        small[bit + 1] = small_next(bit)
-        if bit + 1 < bits_sp:
-            small_copy(bit + 1).start()
-    ring_step(3, late)
-
-    for_early = 4
-
-    def both(k, _):
-        ring_step(k, everything)
-
-    lax.fori_loop(for_early, sp - 2, both, None)
+        if bit < bits_sp:
+            small_copy(bit).wait_recv()
+            small[bit + 1] = small[bit] + small_recv[bit]
+            if bit + 1 < bits_sp:
+                small_copy(bit + 1).start()
+
+    def taps_half(lows):
+        for low in lows:
+            taps_grad(low)
+
+    pair_sums()
+    fixed = min(sp - 2, 6)
+    for k in range(1, fixed + 1):
+        ring_step(k, late)
+        if k + 2 <= sp - 2:
+            ring_step(k + 2, early)
+        if k == 1:
+            taps_half((0, 2))
+        if k == 2:
+            taps_half((4, 6))
+            small_first()
+        if k > 2:
+            small_next(k - 3)
+    for bit in range(max(fixed - 2, 0), bits_sp):
+        small_next(bit)
+    if sp - 2 > fixed:
+
+        def both(k, _):
+            ring_step(k, late)
+            ring_step(k + 2, early)
+
+        lax.fori_loop(fixed + 1, sp - 3, both, None)
+        ring_step(sp - 3, late)
+        ring_step(sp - 2, late)
 
     for bit in range(1, bits_dp):
-        y_copy(bit).wait_recv()
-
-        def add(here, bit=bit):
+        for g in range(GROUPS):
+            y_copy(bit, g).wait_recv()
+            here = of_group(g)
             got = ig_sum[bit - 1, :, here].astype(F32) + ig_peer[bit - 1, :, here].astype(F32)
             ig_sum[bit, :, here] = got.astype(BF16)
-
-        wide_loop(add)
-        if bit + 1 < bits_dp:
-            y_copy(bit + 1).start()
-
-    final = bits_dp - 1
-    give = ig_copy(
-        bits_dp, ig_sum.at[final], ig_out.at[pl.ds(mine, half)], 0
-    )
-    give.start()
-    ring_step(sp - 2, everything)
-
-    def keep(here):
-        ig_out[pl.ds(mine, half), here] = ig_sum[final, :, here]
-
-    wide_loop(keep)
+            if bit + 1 < bits_dp:
+                y_copy(bit + 1, g).start()
+            else:
+                give_copy(g).start()
+    if bits_dp == 1:
+        for g in range(GROUPS):
+            give_copy(g).start()
+    ig_out[pl.ds(mine, half), :] = ig_sum[final]
     small_out[...] = small[bits_sp]
-    outs = (vg_out, gg_out, dg_out)
-    ring_end(everything, outs)
-
-    copy0.wait_send()
-    for bit in range(1, bits_dp):
-        y_copy(bit).wait_send()
-    give.wait()
+    ring_end(early + late, (vg_out, gg_out, dg_out))
+
+    for g in range(GROUPS):
+        pair_copy(g).wait_send()
+        for bit in range(1, bits_dp):
+            y_copy(bit, g).wait_send()
+        give_copy(g).wait()
     for bit in range(bits_sp):
         small_copy(bit).wait_send()
 
     def drain(k, _):
-        for stream in everything:
+        for stream in early + late:
             ring_copy(stream, k).wait_send()
 
     lax.fori_loop(0, sp - 1, drain, None)
 
 
-def finish(ig, vg, gg, dgrad, small, ig_o, vg_o, gg_o, dg_o, k_o, b_o, g_o, s_o, sem):
-    copies = [
-        pltpu.make_async_copy(src, dst, sem.at[at])
-        for at, (src, dst) in enumerate([(ig, ig_o), (vg, vg_o), (gg, gg_o)])
-    ]
-    for copy in copies:
-        copy.start()
+def finish(
+    wide, ig, vg, gg, dgrad, small, ig_o, vg_o, gg_o, dg_o, k_o, b_o, g_o, s_o,
+    t0, t1, k_v, b_v, g_v, s_v, sem,
+):
+    copies = []
+
+    def send(src, dst):
+        copies.append(pltpu.make_async_copy(src, dst, sem.at[len(copies)]))
+        copies[-1].start()
+
+    send(ig, ig_o)
+    turn = [(vg, vg_o), (gg, gg_o)] if wide else [(dgrad, dg_o)]
+    keep = [(dgrad, dg_o)] if wide else [(vg, vg_o), (gg, gg_o)]
+    for src, dst in keep:
+        send(src, dst)
     taps = k_o.shape[0]
-    dg_o[...] = dgrad[...].T
-    k_o[...] = small[0:taps, :]
-    for at, out in enumerate((b_o, g_o, s_o)):
-        out[...] = small[taps + at, :]
+    k_v[...] = small[0:taps, :]
+    send(k_v, k_o)
+    for at, (held, out) in enumerate(((b_v, b_o), (g_v, g_o), (s_v, s_o))):
+        held[...] = small[taps + at, :]
+        send(held, out)
+    for (src, dst), held in zip(turn, (t0, t1)):
+        held[...] = src[...].T
+        send(held, dst)
     for copy in copies:
         copy.wait()
 
@@ -545,16 +666,20 @@
     vmem = pl.BlockSpec(memory_space=pltpu.VMEM)
     hbm = pl.BlockSpec(memory_space=pltpu.HBM)
     dma = pltpu.SemaphoreType.DMA
+    wide = is_wide(chunk, chans)
+    lines, lanes = (chans, chunk) if wide else (chunk, chans)
+    stat_rows = -(-2 * -(-tokens // 128) // 8) * 8
+    count = 3 * 2 * SUBS
     ig, vg, gg, dgrad, small = pl.pallas_call(
         functools.partial(kernel, sp, dp, ratio),
         out_shape=(
             pltpu.VMEM((tokens, width), BF16),
-            pltpu.VMEM((chunk, chans), F32),
-            pltpu.VMEM((chunk, chans), F32),
-            pltpu.VMEM((chunk, chans), F32),
+            pltpu.VMEM((lines, lanes), F32),
+            pltpu.VMEM((lines, lanes), F32),
+            pltpu.VMEM((lines, lanes), F32),
             pltpu.VMEM((small_rows, chans), F32),
         ),
-        in_specs=[hbm] * 5 + [vmem] * 4,
+        in_specs=[hbm] * 9,
         out_specs=(vmem,) * 5,
         scratch_shapes=[
             pltpu.VMEM((tokens, width), BF16),
@@ -562,7 +687,11 @@
             pltpu.VMEM((width, chans), BF16),
             pltpu.VMEM((width, chans), BF16),
             pltpu.VMEM((chans, width), BF16),
-            dma((5,)),
+            pltpu.VMEM((taps, chans), F32),
+            pltpu.VMEM((1, chans), F32),
+            pltpu.VMEM((1, chans), F32),
+            pltpu.VMEM((1, chans), F32),
+            dma((9,)),
             pltpu.VMEM(full, F32),
             pltpu.VMEM(full, F32),
             pltpu.VMEM((tokens + 2 * PAD, chans), F32),
@@ -572,12 +701,13 @@
             pltpu.VMEM(full, BF16),
             pltpu.VMEM(full, BF16),
             pltpu.VMEM(full, BF16),
+            pltpu.VMEM((3, chans, tokens), BF16),
             pltpu.VMEM((2, tokens, 128), F32),
-            pltpu.VMEM((dp, 8, tokens), F32),
-            pltpu.VMEM((dp, 8, tokens), F32),
-            pltpu.VMEM((3, width, chans), F32),
-            pltpu.VMEM((6, sp - 1, chunk // 2, chans), BF16),
-            pltpu.VMEM((6, sp - 1, chunk // 2, chans), BF16),
+            pltpu.VMEM((dp, stat_rows, 128), F32),
+            pltpu.VMEM((dp, stat_rows, 128), F32),
+            pltpu.VMEM((3, sp * lines, lanes), F32),
+            pltpu.VMEM((count, sp - 1, lines // (2 * SUBS), lanes), BF16),
+            pltpu.VMEM((count, sp - 1, lines // (2 * SUBS), lanes), BF16),
             pltpu.VMEM((half, width), BF16),
             pltpu.VMEM((half, width), BF16),
             pltpu.VMEM((half, width), F32),
@@ -589,10 +719,10 @@
             dma((4,)),
             dma((2 * dp,)),
             dma((2 * dp,)),
-            dma((6, sp - 1)),
-            dma((6, sp - 1)),
-            dma((bits_dp + 1,)),
-            dma((bits_dp + 1,)),
+            dma((count, sp - 1)),
+            dma((count, sp - 1)),
+            dma((bits_dp + 1, GROUPS)),
+            dma((bits_dp + 1, GROUPS)),
             dma((bits_sp,)),
             dma((bits_sp,)),
         ],
@@ -612,7 +742,7 @@
     )
     row = jax.ShapeDtypeStruct((chans,), F32)
     return pl.pallas_call(
-        finish,
+        functools.partial(finish, wide),
         out_shape=(
             jax.ShapeDtypeStruct(ig.shape, BF16),
             jax.ShapeDtypeStruct(vg.shape, F32),
@@ -624,8 +754,16 @@
             row,
         ),
         in_specs=[vmem] * 5,
-        out_specs=(hbm,) * 3 + (vmem,) * 5,
-        scratch_shapes=[dma((3,))],
+        out_specs=(hbm,) * 8,
+        scratch_shapes=[
+            pltpu.VMEM((lanes, lines), F32),
+            pltpu.VMEM((lanes, lines), F32),
+            pltpu.VMEM((taps, chans), F32),
+            pltpu.VMEM((chans,), F32),
+            pltpu.VMEM((chans,), F32),
+            pltpu.VMEM((chans,), F32),
+            dma((8,)),
+        ],
         compiler_params=pltpu.CompilerParams(vmem_limit_bytes=FINISH),
     )(ig, vg, gg, dgrad, small)
 

time: 67.7 us -> 56 us (0.83)
  Pallas kernels: 66.8 us -> 55.2 us
    pallas_call x1, Pallas kernels: 64.9 us -> 53.8 us  [on_device(): pl.pallas_call(functools.partial(kernel, sp, dp, ratio), out_shape=(pltpu...]
where the time goes in v1:
time: 56 us; the launch traced here: 55.9 us
  Pallas kernels  55.2 us (99%)
  between operations  0.64 us (1%)
    pallas_call x1, Pallas kernels, on_device(): pl.pallas_call(functools.partial(kernel, sp, dp, ratio), out_shape=(pltpu...  53.8 us
    pallas_call x1, Pallas kernels, on_device(): pl.pallas_call(functools.partial(finish, wide), out_shape=(jax.ShapeDtype...  1.4 us

profile of v1, /device:TPU:0, one launch (start us, length us, event | category | flops | bytes accessed | tf_op | source)
XLA Modules:
  0.0 55.9 jit_solution(16617423770407978823)
XLA Ops:
  0.6 53.8 %shard_map.152 = (bf16[320,2048]{1,0:T(8,128)(2,1)S(1)}, f32[256,256]{1,0:T(8,128)S(1)}, f32[256,256]{1,0:T(8,128)S(1)}, f32[256,256]{1,0:T(8,128)S(1)}, f32[40,256]{1,0:T(8,128)S(1)}) custom-call(bf16[320,2048]{1,0:T(8,128)(2,1)} %x_hbm.1, bf16[320,2048]{1,0:T(8,128)(2,1)} %og_hbm.1, bf16[2048,256]{1,0:T(8,128)(2,1)} %wv_hbm.1, bf16[2048,256]{1,0:T(8,128)(2,1)} %wg_hbm.1, ...), custom_call_target="tpu_custom_call" | custom-call | tf_op jit(solution)/shard_map/pallas_call | solution.py:673
  54.5 1.4 %shard_map.153 = (bf16[320,2048]{1,0:T(8,128)(2,1)}, f32[256,256]{1,0:T(8,128)}, f32[256,256]{1,0:T(8,128)}, f32[256,256]{1,0:T(8,128)}, f32[31,256]{1,0:T(8,128...) custom-call(bf16[320,2048]{1,0:T(8,128)(2,1)S(1)} %get-tuple-element.13.ig, f32[256,256]{1,0:T(8,128)S(1)} %get-tuple-element.14.vg, ...), custom_call_target="tpu_custom_call" | custom-call | tf_op jit(solution)/shard_map/pallas_call | solution.py:744

commit v2 on v1

--- a/solution.py
+++ b/solution.py
@@ -18,7 +18,7 @@
 PAD = 16
 ROWS = 32
 SUBS = 2
-GROUPS = 4
+GROUPS = 2
 MAIN = 61_900_000
 FINISH = 16_000_000
 
@@ -78,7 +78,6 @@
     turned,
     cols,
     stats,
-    stats2,
     part,
     ring_src,
     ring_dst,
@@ -97,6 +96,7 @@
     ring_recv,
     ig_ssem,
     ig_rsem,
+    give_rsem,
     small_ssem,
     small_rsem,
 ):
@@ -156,43 +156,46 @@
             barrier, inc=1, device_id={"dp": lax.rem(d + off, dp)}, device_id_type=MESH
         )
 
-    loads[0].wait()
-    loads[1].wait()
-    value[...] = dot(x[...], wv[...], NN).astype(BF16).astype(F32)
-    loads[2].wait()
-    opening[...] = dot(x[...], wg[...], NN).astype(BF16).astype(F32)
-
-    def row_loop(fn, init=None, rows=ROWS):
+    for load in loads[:3]:
+        load.wait()
+    value_f, gate_f = dot(x[...], wv[...], NN), dot(x[...], wg[...], NN)
+    value[...] = value_f.astype(BF16).astype(F32)
+    opening[...] = gate_f.astype(BF16).astype(F32)
+
+    def row_loop(fn, init=None, rows=ROWS, begin=0, end=tokens):
         def step(i, carry):
-            return fn(pl.multiple_of(i * rows, rows), carry)
-
-        return lax.fori_loop(0, tokens // rows, step, init)
-
-    big = 80 if tokens % 80 == 0 else ROWS
+            return fn(pl.multiple_of(begin + i * rows, math.gcd(begin, rows)), carry)
+
+        return lax.fori_loop(0, (end - begin) // rows, step, init)
+
+    ext = tokens + 2 * PAD
+    inner_rows = ext - 2 * ROWS
+    big = 96 if inner_rows % 96 == 0 else ROWS
+    own = pl.ds(PAD, tokens)
 
     def make_glu(r, _):
         here = pl.ds(r, ROWS)
         o = jax.nn.sigmoid(opening[here, :])
         opening[here, :] = o
-        glu[pl.ds(r + PAD, ROWS), :] = value[here, :] * o
+        glu[pl.ds(r + 2 * PAD, ROWS), :] = value[here, :] * o
 
     row_loop(make_glu)
     pl.semaphore_wait(barrier, len(peers) + dp - 1)
 
     has_low, has_high = s > 0, s < sp - 1
 
-    def halo_copies(buf, at):
+    def halo_copies(buf, pad, at):
         up = pltpu.make_async_remote_copy(
-            src_ref=buf.at[pl.ds(tokens, PAD)],
-            dst_ref=buf.at[pl.ds(0, PAD)],
+            src_ref=buf.at[pl.ds(tokens, pad)],
+            dst_ref=buf.at[pl.ds(0, pad)],
             send_sem=halo_send.at[at],
             recv_sem=halo_recv.at[at],
             device_id={"sp": lax.rem(s + 1, sp)},
             device_id_type=MESH,
         )
         down = pltpu.make_async_remote_copy(
-            src_ref=buf.at[pl.ds(PAD, PAD)],
-            dst_ref=buf.at[pl.ds(tokens + PAD, PAD)],
+            src_ref=buf.at[pl.ds(pad, pad)],
+            dst_ref=buf.at[pl.ds(tokens + pad, pad)],
             send_sem=halo_send.at[at + 1],
             recv_sem=halo_recv.at[at + 1],
             device_id={"sp": lax.rem(s + sp - 1, sp)},
@@ -200,21 +203,23 @@
         )
         return up, down
 
-    def halo_start(buf, at):
-        up, down = halo_copies(buf, at)
+    def halo_zero(buf, pad):
+        @pl.when(s == 0)
+        def _():
+            buf[pl.ds(0, pad), :] = jnp.zeros((pad, chans), F32)
+
+        @pl.when(s == sp - 1)
+        def _():
+            buf[pl.ds(tokens + pad, pad), :] = jnp.zeros((pad, chans), F32)
+
+    def halo_start(buf, pad, at):
+        up, down = halo_copies(buf, pad, at)
         pl.when(has_high)(up.start)
         pl.when(has_low)(down.start)
-
-        @pl.when(s == 0)
-        def _():
-            buf[pl.ds(0, PAD), :] = jnp.zeros((PAD, chans), F32)
-
-        @pl.when(s == sp - 1)
-        def _():
-            buf[pl.ds(tokens + PAD, PAD), :] = jnp.zeros((PAD, chans), F32)
-
-    def halo_wait(buf, at):
-        up, down = halo_copies(buf, at)
+        halo_zero(buf, pad)
+
+    def halo_wait(buf, pad, at):
+        up, down = halo_copies(buf, pad, at)
 
         @pl.when(has_low)
         def _():
@@ -226,23 +231,11 @@
             down.wait_recv()
             up.wait_send()
 
-    def inner_outer(fn, between):
-        blocks = tokens // ROWS
-
-        def inner(i, _):
-            fn(pl.multiple_of(i * ROWS, ROWS), None)
-
-        def outer(i, _):
-            fn(pl.multiple_of(i * (blocks - 1) * ROWS, ROWS), None)
-
-        lax.fori_loop(1, blocks - 1, inner, None)
-        between()
-        lax.fori_loop(0, 2, outer, None)
-
-    halo_start(glu, 0)
+    halo_start(glu, 2 * PAD, 0)
     for load in loads[3:]:
         load.wait()
-    d_act[...] = dot(og[...], wd[...], NT)
+    d_act[own, :] = dot(og[...], wd[...], NT)
+    halo_start(d_act, PAD, 2)
 
     span = ROWS + 2 * PAD
 
@@ -264,66 +257,109 @@
         acc = jnp.zeros((ROWS, chans), F32) + bias[...]
         mixed[pl.ds(r, ROWS), :] = slide(glu, r, lambda tap: tap + PAD - reach, acc)
 
-    inner_outer(conv, lambda: halo_wait(glu, 0))
-
     ones = jnp.ones((16, chans), BF16)
-    line = lax.broadcasted_iota(jnp.int32, (8, tokens), 0)
     eye = (
         lax.rem(lax.broadcasted_iota(jnp.int32, (24, 128), 0), 8)
         == lax.broadcasted_iota(jnp.int32, (24, 128), 1)
     ).astype(BF16)
-    pieces = [(at, min(128, tokens - at)) for at in range(0, tokens, 128)]
+    edges = ((0, ROWS), (ext - ROWS, ROWS))
+    regions = (((ROWS, inner_rows),), edges)
+
+    def pieces_of(region):
+        count = sum(size for _, size in regions[region])
+        return [(at, min(128, count - at)) for at in range(0, count, 128)]
+
+    def rows_of(buf, region):
+        got = [buf[pl.ds(first, size), :] for first, size in regions[region]]
+        return got[0] if len(got) == 1 else jnp.concatenate(got, axis=0)
 
     def row_sums(v):
         a, b, c = (dot(ones, term, NT) for term in split3(v))
         return a + b + c
 
-    def columns(one, two):
+    def columns(at, region, one, two):
+        line = lax.broadcasted_iota(jnp.int32, (8, one.shape[1]), 0)
         both = jnp.where(line == 0, one, jnp.where(line == 1, two, 0.0))
         terms = [term.astype(F32) for term in split3(both)]
-        return dot(jnp.concatenate(terms, axis=0).astype(BF16), eye, TN)
-
-    def stat_copy(buf, off, at):
+        got = dot(jnp.concatenate(terms, axis=0).astype(BF16), eye, TN)
+        done = 0
+        for first, size in regions[region]:
+            cols[at, pl.ds(first, size), :] = got[done : done + size]
+            done += size
+
+    def stat_copy(at, off):
         return pltpu.make_async_remote_copy(
-            src_ref=buf.at[0],
-            dst_ref=buf.at[off],
-            send_sem=stat_send.at[at * dp + off],
-            recv_sem=stat_recv.at[at * dp + off],
+            src_ref=stats.at[at, 0],
+            dst_ref=stats.at[at, off],
+            send_sem=stat_send.at[at],
+            recv_sem=stat_recv.at[at],
             device_id={"dp": lax.rem(d + off, dp)},
             device_id_type=MESH,
         )
 
-    def stat_start(buf, at, one, two):
-        buf[0] = jnp.zeros(buf.shape[1:], F32)
+    def stat_all(at):
+        every = stats.at[at, pl.ds(1, dp - 1)]
+        return pltpu.make_async_remote_copy(
+            src_ref=every,
+            dst_ref=every,
+            send_sem=stat_send.at[at],
+            recv_sem=stat_recv.at[at],
+            device_id={"dp": lax.rem(d + 1, dp)},
+            device_id_type=MESH,
+        )
+
+    def stat_start(at, region, one, two):
+        pieces = pieces_of(region)
+        stats[at, 0] = jnp.zeros(stats.shape[2:], F32)
         for first, sums in ((0, row_sums(one)), (len(pieces), row_sums(two))):
             for j, (begin, size) in enumerate(pieces):
-                buf[0, first + j : first + j + 1, 0:size] = sums[0:1, begin : begin + size]
+                stats[at, 0, first + j : first + j + 1, 0:size] = sums[0:1, begin : begin + size]
         for off in range(1, dp):
-            stat_copy(buf, off, at).start()
-
-    def stat_wait(buf, at):
+            stat_copy(at, off).start()
+
+    def stat_wait(at, region):
+        pieces = pieces_of(region)
+        stat_all(at).wait_recv()
+        total = stats[at, 0]
         for off in range(1, dp):
-            stat_copy(buf, off, at).wait()
-        total = buf[0]
-        for off in range(1, dp):
-            total = total + buf[off]
+            total = total + stats[at, off]
         total = total * (1.0 / channels)
-        one, two = (
+        return tuple(
             jnp.concatenate(
                 [total[first + j : first + j + 1, 0:size] for j, (_, size) in enumerate(pieces)],
                 axis=1,
             )
             for first in (0, len(pieces))
         )
-        return one, two
-
-    stat_start(stats, 0, mixed[...], mixed[...] * mixed[...])
-    mean, square = stat_wait(stats, 0)
-    cols[0] = columns(mean, lax.rsqrt(square - mean * mean + EPS))
-
-    def norm(r, carry):
-        gain_sum, shift_sum = carry
-        here = pl.ds(r, big)
+
+    def moments_start(region):
+        v = rows_of(mixed, region)
+        stat_start(region, region, v, v * v)
+
+    def moments_wait(region):
+        mean, square = stat_wait(region, region)
+        columns(0, region, mean, lax.rsqrt(square - mean * mean + EPS))
+
+    def second_start(region):
+        v = rows_of(d_act, region)
+        stat_start(2 + region, region, v, v * rows_of(mixed, region))
+
+    def second_wait(region):
+        columns(1, region, *stat_wait(2 + region, region))
+
+    row_loop(conv, begin=ROWS, end=ext - ROWS)
+    moments_start(0)
+    halo_wait(glu, 2 * PAD, 0)
+
+    def conv_edge(i, _):
+        conv(pl.multiple_of(i * (ext - ROWS), ROWS), None)
+
+    lax.fori_loop(0, 2, conv_edge, None)
+    moments_start(1)
+    halo_wait(d_act, PAD, 2)
+
+    def norm_rows(r, rows):
+        here = pl.ds(r, rows)
         col = cols[0, here, :]
         centred = (mixed[here, :] - col[:, 0:1]) * col[:, 1:2]
         normed = centred * gain[...] + shift[...]
@@ -332,13 +368,24 @@
         d_normed = d_act[here, :] * sig * (1.0 + normed * (1.0 - sig))
         mixed[here, :] = centred
         d_act[here, :] = d_normed * gain[...]
-        gain_sum = gain_sum + jnp.sum(d_normed * centred, axis=0, keepdims=True)
-        shift_sum = shift_sum + jnp.sum(d_normed, axis=0, keepdims=True)
-        return gain_sum, shift_sum
+        return d_normed * centred, d_normed
+
+    def down(v):
+        return jnp.sum(v, axis=0, keepdims=True)
+
+    def norm(r, carry):
+        return tuple(had + down(v) for had, v in zip(carry, norm_rows(r, big)))
 
     zero = jnp.zeros((1, chans), F32)
-    gain_sum, shift_sum = row_loop(norm, (zero, zero), big)
-    stat_start(stats2, 1, d_act[...], d_act[...] * mixed[...])
+    moments_wait(0)
+    sums = row_loop(norm, (zero, zero), big, ROWS, ext - ROWS)
+    second_start(0)
+    moments_wait(1)
+    kept = (slice(PAD, ROWS), slice(0, ROWS - PAD))
+    for (first, size), keep in zip(edges, kept):
+        sums = tuple(had + down(v[keep]) for had, v in zip(sums, norm_rows(first, size)))
+    gain_sum, shift_sum = sums
+    second_start(1)
 
     def several(count, fn):
         if count <= 8:
@@ -356,14 +403,14 @@
 
     def grad_first(at, rows, factor):
         if wide:
-            turned[at] = factor[...].T
+            turned[at] = factor.T
             grad_tile(at, rows, -1)
             grad_tile(at, rows, 1)
             return
 
         def step(i, _):
             here = pl.ds(pl.multiple_of(i * tile, tile), tile)
-            part[at, here, :] = dot(rows[:, here], factor[...], TN)
+            part[at, here, :] = dot(rows[:, here], factor, TN)
 
         lax.fori_loop(0, width // tile, step, None)
 
@@ -389,7 +436,7 @@
         return pltpu.make_async_remote_copy(
             src_ref=ring_src.at[stream, k],
             dst_ref=ring_dst.at[stream, k],
-            send_sem=ring_send.at[stream, k],
+            send_sem=ring_send.at[0],
             recv_sem=ring_recv.at[stream, k],
             device_id={"sp": ahead if streams[stream][2] == 1 else behind},
             device_id_type=MESH,
@@ -413,23 +460,26 @@
                 piece(stream, pos) + ring_dst[stream, sp - 2].astype(F32)
             )
 
-    grad_first(2, og, act)
+    grad_first(2, og, act[own, :])
     ring_step(0, early)
     grad_rest(2, og)
 
-    first, second = stat_wait(stats2, 1)
-    cols[1] = columns(first, second)
-
-    def norm_back(r, bias_sum):
-        here = pl.ds(r, big)
+    def back_rows(r, rows):
+        here = pl.ds(r, rows)
         col, back = cols[0, here, :], cols[1, here, :]
         d_mixed = col[:, 1:2] * (d_act[here, :] - back[:, 0:1] - mixed[here, :] * back[:, 1:2])
-        d_pad[pl.ds(r + PAD, big), :] = d_mixed
-        return bias_sum + jnp.sum(d_mixed, axis=0, keepdims=True)
-
-    bias_sum = row_loop(norm_back, zero, big)
-    halo_start(d_pad, 2)
-    ring_step(1, early)
+        d_pad[here, :] = d_mixed
+        return d_mixed
+
+    def norm_back(r, bias_sum):
+        return bias_sum + down(back_rows(r, big))
+
+    second_wait(0)
+    bias_sum = row_loop(norm_back, zero, big, ROWS, ext - ROWS)
+    second_wait(1)
+    for (first, size), keep in zip(edges, kept):
+        bias_sum = bias_sum + down(back_rows(first, size)[keep])
+    halo_zero(d_pad, PAD)
 
     def conv_back(r, _):
         here = pl.ds(r, ROWS)
@@ -440,10 +490,13 @@
         dv[here, :] = grad.astype(BF16)
         dg[here, :] = (grad * value[here, :] * (1.0 - o)).astype(BF16)
 
-    inner_outer(conv_back, lambda: halo_wait(d_pad, 2))
-    grad_first(0, x, dv)
+    middle = tokens // ROWS // 2 * ROWS
+    row_loop(conv_back, end=middle)
+    ring_step(1, early)
+    row_loop(conv_back, begin=middle)
+    grad_first(0, x, dv[...])
     ring_step(0, late_of(0))
-    grad_first(1, x, dg)
+    grad_first(1, x, dg[...])
     ring_step(0, late_of(1))
     grad_rest(0, x)
     grad_rest(1, x)
@@ -458,8 +511,8 @@
         return pltpu.make_async_remote_copy(
             src_ref=src,
             dst_ref=dst,
-            send_sem=ig_ssem.at[at, g],
-            recv_sem=ig_rsem.at[at, g],
+            send_sem=ig_ssem.at[at],
+            recv_sem=give_rsem.at[0] if at == bits_dp else ig_rsem.at[at, g],
             device_id={"dp": flip(d, bit)},
             device_id_type=MESH,
         )
@@ -516,7 +569,7 @@
             grad = d_pad[pl.ds(r + PAD, ROWS), :]
             new = []
             for at in range(2):
-                window = shifted(glu, r, low + at)
+                window = shifted(glu, r + PAD, low + at)
                 for tap in those[at]:
                     high = tap + PAD - reach - low - at
                     prod = grad * window[high : high + ROWS]
@@ -535,7 +588,7 @@
         return pltpu.make_async_remote_copy(
             src_ref=small.at[bit],
             dst_ref=small_recv.at[bit],
-            send_sem=small_ssem.at[bit],
+            send_sem=small_ssem.at[0],
             recv_sem=small_rsem.at[bit],
             device_id={"sp": flip(s, bit)},
             device_id_type=MESH,
@@ -600,19 +653,29 @@
     small_out[...] = small[bits_sp]
     ring_end(early + late, (vg_out, gg_out, dg_out))
 
-    for g in range(GROUPS):
-        pair_copy(g).wait_send()
-        for bit in range(1, bits_dp):
-            y_copy(bit, g).wait_send()
-        give_copy(g).wait()
-    for bit in range(bits_sp):
-        small_copy(bit).wait_send()
-
-    def drain(k, _):
-        for stream in early + late:
-            ring_copy(stream, k).wait_send()
-
-    lax.fori_loop(0, sp - 1, drain, None)
+    ig_copy(0, 0, ig_send, ig_recv, 0).wait_send()
+    for bit in range(1, bits_dp):
+        ig_copy(bit, 0, ig_sum.at[bit - 1], ig_peer.at[bit - 1], bit).wait_send()
+    ig_copy(bits_dp, 0, ig_sum.at[final], ig_out.at[pl.ds(mine, half)], 0).wait()
+    for at in range(4):
+        stat_all(at).wait_send()
+    rounds = small.at[pl.ds(0, bits_sp)]
+    pltpu.make_async_remote_copy(
+        src_ref=rounds,
+        dst_ref=rounds,
+        send_sem=small_ssem.at[0],
+        recv_sem=small_rsem.at[0],
+        device_id={"sp": flip(s, 0)},
+        device_id_type=MESH,
+    ).wait_send()
+    pltpu.make_async_remote_copy(
+        src_ref=ring_src,
+        dst_ref=ring_dst,
+        send_sem=ring_send.at[0],
+        recv_sem=ring_recv.at[0, 0],
+        device_id={"sp": ahead},
+        device_id_type=MESH,
+    ).wait_send()
 
 
 def finish(
@@ -662,7 +725,7 @@
     bits_sp, bits_dp = sp.bit_length() - 1, dp.bit_length() - 1
     small_rows = -(-(taps + 3) // 8) * 8
     half = tokens // 2
-    full = (tokens, chans)
+    full, extended = (tokens, chans), (tokens + 2 * PAD, chans)
     vmem = pl.BlockSpec(memory_space=pltpu.VMEM)
     hbm = pl.BlockSpec(memory_space=pltpu.HBM)
     dma = pltpu.SemaphoreType.DMA
@@ -694,17 +757,16 @@
             dma((9,)),
             pltpu.VMEM(full, F32),
             pltpu.VMEM(full, F32),
-            pltpu.VMEM((tokens + 2 * PAD, chans), F32),
-            pltpu.VMEM(full, F32),
-            pltpu.VMEM(full, F32),
-            pltpu.VMEM((tokens + 2 * PAD, chans), F32),
-            pltpu.VMEM(full, BF16),
+            pltpu.VMEM((tokens + 4 * PAD, chans), F32),
+            pltpu.VMEM(extended, F32),
+            pltpu.VMEM(extended, F32),
+            pltpu.VMEM(extended, F32),
+            pltpu.VMEM(extended, BF16),
             pltpu.VMEM(full, BF16),
             pltpu.VMEM(full, BF16),
             pltpu.VMEM((3, chans, tokens), BF16),
-            pltpu.VMEM((2, tokens, 128), F32),
-            pltpu.VMEM((dp, stat_rows, 128), F32),
-            pltpu.VMEM((dp, stat_rows, 128), F32),
+            pltpu.VMEM((2, tokens + 2 * PAD, 128), F32),
+            pltpu.VMEM((4, dp, stat_rows, 128), F32),
             pltpu.VMEM((3, sp * lines, lanes), F32),
             pltpu.VMEM((count, sp - 1, lines // (2 * SUBS), lanes), BF16),
             pltpu.VMEM((count, sp - 1, lines // (2 * SUBS), lanes), BF16),
@@ -717,13 +779,14 @@
             pltpu.VMEM((bits_sp, small_rows, chans), F32),
             dma((4,)),
             dma((4,)),
-            dma((2 * dp,)),
-            dma((2 * dp,)),
+            dma((4,)),
+            dma((4,)),
+            dma((1,)),
             dma((count, sp - 1)),
-            dma((count, sp - 1)),
-            dma((bits_dp + 1, GROUPS)),
-            dma((bits_dp + 1, GROUPS)),
-            dma((bits_sp,)),
+            dma((bits_dp + 1,)),
+            dma((bits_dp, GROUPS)),
+            dma((1,)),
+            dma((1,)),
             dma((bits_sp,)),
         ],
         compiler_params=pltpu.CompilerParams(

time: 56 us -> 53.3 us (0.952)
  Pallas kernels: 55.2 us -> 52.5 us
    pallas_call x1, Pallas kernels: 53.8 us -> 51.1 us  [on_device(): pl.pallas_call(functools.partial(kernel, sp, dp, ratio), out_shape=(pltpu...]
where the time goes in v2:
time: 53.3 us; the launch traced here: 53.1 us
  Pallas kernels  52.5 us (98%)
  between operations  0.64 us (1%)
    pallas_call x1, Pallas kernels, on_device(): pl.pallas_call(functools.partial(kernel, sp, dp, ratio), out_shape=(pltpu...  51.1 us
    pallas_call x1, Pallas kernels, on_device(): pl.pallas_call(functools.partial(finish, wide), out_shape=(jax.ShapeDtype...  1.4 us

profile of v2, /device:TPU:0, one launch (start us, length us, event | category | flops | bytes accessed | tf_op | source)
XLA Modules:
  0.0 53.1 jit_solution(6026478962171789337)
XLA Ops:
  0.6 51.1 %shard_map.152 = (bf16[320,2048]{1,0:T(8,128)(2,1)S(1)}, f32[256,256]{1,0:T(8,128)S(1)}, f32[256,256]{1,0:T(8,128)S(1)}, f32[256,256]{1,0:T(8,128)S(1)}, f32[40,256]{1,0:T(8,128)S(1)}) custom-call(bf16[320,2048]{1,0:T(8,128)(2,1)} %x_hbm.1, bf16[320,2048]{1,0:T(8,128)(2,1)} %og_hbm.1, bf16[2048,256]{1,0:T(8,128)(2,1)} %wv_hbm.1, bf16[2048,256]{1,0:T(8,128)(2,1)} %wg_hbm.1, ...), custom_call_target="tpu_custom_call" | custom-call | tf_op jit(solution)/shard_map/pallas_call | solution.py:736
  51.7 1.4 %shard_map.153 = (bf16[320,2048]{1,0:T(8,128)(2,1)}, f32[256,256]{1,0:T(8,128)}, f32[256,256]{1,0:T(8,128)}, f32[256,256]{1,0:T(8,128)}, f32[31,256]{1,0:T(8,128...) custom-call(bf16[320,2048]{1,0:T(8,128)(2,1)S(1)} %get-tuple-element.13.ig, f32[256,256]{1,0:T(8,128)S(1)} %get-tuple-element.14.vg, ...), custom_call_target="tpu_custom_call" | custom-call | tf_op jit(solution)/shard_map/pallas_call | solution.py:807

commit v3 on v2

--- a/solution.py
+++ b/solution.py
@@ -36,6 +36,10 @@
 
 def is_wide(chunk, chans):
     return chunk % 128 == 0 and chans % 32 == 0
+
+
+def is_paired(sp, dp, chunk, chans):
+    return is_wide(chunk, chans) and chans % 256 == 0 and sp % 4 == 0 and sp >= 8 and dp % 2 == 0
 
 
 def kernel(
@@ -99,6 +103,20 @@
     give_rsem,
     small_ssem,
     small_rsem,
+    xp,
+    ogp,
+    in_recv,
+    lhs,
+    x_send,
+    x_recv,
+    held,
+    z_send,
+    z_recv,
+    pair_sends,
+    near_recv,
+    in_rsem,
+    x_rsem,
+    z_rsem,
 ):
     tokens, width = x.shape
     taps, chans = ck.shape
@@ -106,6 +124,7 @@
     reach = taps // 2
     chunk = width // sp
     wide = is_wide(chunk, chans)
+    paired = is_paired(sp, dp, chunk, chans)
     lines = chans if wide else chunk
     strip = lines // (2 * SUBS)
     tile = min(256, width)
@@ -149,6 +168,9 @@
     barrier = pltpu.get_barrier_semaphore()
     peers = [ahead, behind, lax.rem(s + 1, sp), lax.rem(s + sp - 1, sp)]
     peers += [flip(s, bit) for bit in range(bits_sp)]
+    quads = sp // 4
+    if paired and quads > 2:
+        peers += [lax.rem(s + 4 * far, sp) for far in range(1, quads)]
     for peer in peers:
         pl.semaphore_signal(barrier, inc=1, device_id={"sp": peer}, device_id_type=MESH)
     for off in range(1, dp):
@@ -231,11 +253,59 @@
             down.wait_recv()
             up.wait_send()
 
+    half = tokens // 2
+    hand = chans // 2
+    core = lax.rem(d, 2)
+    these = pl.ds(pl.multiple_of(core * half, half), half)
+    slots = [(far, other) for other in (1, 0) for far in range(quads)]
+    held_rows, near_rows = (x, og), (xp, ogp)
+    in_bits, mid_bits = (1, 0), (0, 1)
+
+    def columns_of(who, far, other, kind):
+        index = lax.rem(who + 4 * far, sp)
+        if other:
+            index = flip(index, mid_bits[kind])
+        return pl.ds(pl.multiple_of(index * chunk, chunk), chunk)
+
+    def slot_of(far, other):
+        return pl.ds((2 * far + other) * chunk, chunk)
+
+    def send_to(at, src, dst, recv_sem, where):
+        return pltpu.make_async_remote_copy(
+            src_ref=src,
+            dst_ref=dst,
+            send_sem=pair_sends.at[at],
+            recv_sem=recv_sem,
+            device_id=where,
+            device_id_type=MESH,
+        )
+
+    def near_start(kind, those):
+        there = flip(s, in_bits[kind])
+        for far, other in those if paired else ():
+            send_to(
+                kind,
+                held_rows[kind].at[these, columns_of(there, far, other, kind)],
+                near_rows[kind].at[these, slot_of(far, other)],
+                near_recv.at[kind],
+                {"sp": there},
+            ).start()
+
+    def near_all(kind, stage):
+        where = {"dp": flip(d, 0)} if stage else {"sp": flip(s, in_bits[kind])}
+        rows = near_rows[kind].at[these]
+        at = kind + 2 * stage
+        return send_to(at, rows, rows, near_recv.at[at], where)
+
     halo_start(glu, 2 * PAD, 0)
+    near_start(0, slots[:1])
     for load in loads[3:]:
         load.wait()
+    near_start(1, slots[:1])
     d_act[own, :] = dot(og[...], wd[...], NT)
     halo_start(d_act, PAD, 2)
+    near_start(1, slots[1:])
+    near_start(0, slots[1:])
 
     span = ROWS + 2 * PAD
 
@@ -356,7 +426,6 @@
 
     lax.fori_loop(0, 2, conv_edge, None)
     moments_start(1)
-    halo_wait(d_act, PAD, 2)
 
     def norm_rows(r, rows):
         here = pl.ds(r, rows)
@@ -380,6 +449,7 @@
     moments_wait(0)
     sums = row_loop(norm, (zero, zero), big, ROWS, ext - ROWS)
     second_start(0)
+    halo_wait(d_act, PAD, 2)
     moments_wait(1)
     kept = (slice(PAD, ROWS), slice(0, ROWS - PAD))
     for (first, size), keep in zip(edges, kept):
@@ -460,9 +530,67 @@
                 piece(stream, pos) + ring_dst[stream, sp - 2].astype(F32)
             )
 
-    grad_first(2, og, act[own, :])
-    ring_step(0, early)
-    grad_rest(2, og)
+    blocks = [(at, hand * place) for at in (2, 0, 1) for place in range(2)]
+
+    def kind_of(n):
+        return int(blocks[n][0] == 2)
+
+    def factor_of(n):
+        at, first = blocks[n]
+        those = pl.ds(first, hand)
+        return (dv, dg, act)[at].at[own if at == 2 else pl.ds(0, tokens), those]
+
+    def in_copy(n):
+        where = {"sp": flip(s, in_bits[kind_of(n)])}
+        return send_to(4, factor_of(n), in_recv.at[n], in_rsem.at[n], where)
+
+    def mid_copy(n):
+        where = {"sp": flip(s, mid_bits[kind_of(n)])}
+        return send_to(5, x_send.at[n], x_recv.at[n], x_rsem.at[n], where)
+
+    def far_copy(n, far):
+        where = {"sp": lax.rem(s + 4 * far, sp)}
+        return send_to(
+            6, z_send.at[n, far - 1], z_recv.at[n, far - 1], z_rsem.at[n, far - 1], where
+        )
+
+    def product(n):
+        kind = kind_of(n)
+        in_copy(n).wait_recv()
+        lhs[...] = jnp.concatenate([factor_of(n)[...], in_recv[n]], axis=0).T
+        for far, other in slots:
+            mine = held_rows[kind][:, columns_of(s, far, other, kind)]
+            rows = jnp.concatenate([mine, near_rows[kind][:, slot_of(far, other)]], axis=0)
+            got = dot(lhs[...], rows, NN)
+            if other:
+                x_send[n, far] = got.astype(BF16)
+            else:
+                held[n, far] = got
+            if (far, other) == (quads - 1, 1):
+                mid_copy(n).start()
+
+    def meet(n):
+        mid_copy(n).wait_recv()
+        for far in range(1, quads):
+            z_send[n, far - 1] = (held[n, far] + x_recv[n, far].astype(F32)).astype(BF16)
+            far_copy(n, far).start()
+        held[n, 0] = held[n, 0] + x_recv[n, 0].astype(F32)
+
+    def settle(n, outs):
+        at, first = blocks[n]
+        total = held[n, 0]
+        for far in range(1, quads):
+            far_copy(n, far).wait_recv()
+            total = total + z_recv[n, far - 1].astype(F32)
+        outs[at][pl.ds(first, hand), :] = ratio * total
+
+    if paired:
+        for n in range(2):
+            in_copy(n).start()
+    else:
+        grad_first(2, og, act[own, :])
+        ring_step(0, early)
+        grad_rest(2, og)
 
     def back_rows(r, rows):
         here = pl.ds(r, rows)
@@ -492,17 +620,21 @@
 
     middle = tokens // ROWS // 2 * ROWS
     row_loop(conv_back, end=middle)
-    ring_step(1, early)
+    if not paired:
+        ring_step(1, early)
     row_loop(conv_back, begin=middle)
-    grad_first(0, x, dv[...])
-    ring_step(0, late_of(0))
-    grad_first(1, x, dg[...])
-    ring_step(0, late_of(1))
-    grad_rest(0, x)
-    grad_rest(1, x)
-    ring_step(2, early)
-
-    half = tokens // 2
+    if paired:
+        for n in (2, 3):
+            in_copy(n).start()
+    else:
+        grad_first(0, x, dv[...])
+        ring_step(0, late_of(0))
+        grad_first(1, x, dg[...])
+        ring_step(0, late_of(1))
+        grad_rest(0, x)
+        grad_rest(1, x)
+        ring_step(2, early)
+
     mine = pl.multiple_of(lax.rem(d, 2) * half, half)
     other = pl.multiple_of((1 - lax.rem(d, 2)) * half, half)
     group = width // GROUPS
@@ -538,25 +670,6 @@
             ig_out.at[pl.ds(mine, half), of_group(g)],
             0,
         )
-
-    both_v = jnp.concatenate([dv[pl.ds(other, half), :], dv[pl.ds(mine, half), :]], axis=0)
-    both_g = jnp.concatenate([dg[pl.ds(other, half), :], dg[pl.ds(mine, half), :]], axis=0)
-    size = min(tile, group)
-    for g in range(GROUPS):
-        for begin in range(g * group, (g + 1) * group, size):
-            here = pl.ds(begin, size)
-            got = dot(both_v, wv[here, :], NT) + dot(both_g, wg[here, :], NT)
-            ig_send[:, here] = got[:half].astype(BF16)
-            ig_own[:, here] = got[half:]
-        pair_copy(g).start()
-
-    def pair_sums():
-        for g in range(GROUPS):
-            pair_copy(g).wait_recv()
-            here = of_group(g)
-            ig_sum[0, :, here] = (ig_own[:, here] + ig_recv[:, here].astype(F32)).astype(BF16)
-            if bits_dp > 1:
-                y_copy(1, g).start()
 
     small[0] = jnp.zeros(small.shape[1:], F32)
 
@@ -590,7 +703,7 @@
             dst_ref=small_recv.at[bit],
             send_sem=small_ssem.at[0],
             recv_sem=small_rsem.at[bit],
-            device_id={"sp": flip(s, bit)},
+            device_id={"sp": flip(s, (bit + 1) % bits_sp)},
             device_id_type=MESH,
         )
 
@@ -611,8 +724,56 @@
         for low in lows:
             taps_grad(low)
 
+    both_v = jnp.concatenate([dv[pl.ds(other, half), :], dv[pl.ds(mine, half), :]], axis=0)
+    both_g = jnp.concatenate([dg[pl.ds(other, half), :], dg[pl.ds(mine, half), :]], axis=0)
+    size = min(tile, group)
+    for g in range(GROUPS):
+        for begin in range(g * group, (g + 1) * group, size):
+            here = pl.ds(begin, size)
+            got = dot(both_v, wv[here, :], NT) + dot(both_g, wg[here, :], NT)
+            ig_send[:, here] = got[:half].astype(BF16)
+            ig_own[:, here] = got[half:]
+        pair_copy(g).start()
+
+    def pair_sums():
+        for g in range(GROUPS):
+            pair_copy(g).wait_recv()
+            here = of_group(g)
+            ig_sum[0, :, here] = (ig_own[:, here] + ig_recv[:, here].astype(F32)).astype(BF16)
+            if bits_dp > 1:
+                y_copy(1, g).start()
+
+    if paired:
+        for kind in (1, 0):
+            near_all(kind, 0).wait_recv()
+            near_all(kind, 1).start()
+        taps_half((0, 2, 4, 6))
+        small_first()
+        for n in (4, 5):
+            in_copy(n).start()
     pair_sums()
     fixed = min(sp - 2, 6)
+    if paired:
+        near_all(0, 1).wait_recv()
+        product(2)
+        product(3)
+        small_next(0)
+        near_all(1, 1).wait_recv()
+        product(0)
+        product(1)
+        product(4)
+        product(5)
+        meet(2)
+        small_next(1)
+        meet(3)
+        meet(0)
+        meet(4)
+        meet(1)
+        meet(5)
+        small_next(2)
+        for bit in range(3, bits_sp):
+            small_next(bit)
+        fixed = 0
     for k in range(1, fixed + 1):
         ring_step(k, late)
         if k + 2 <= sp - 2:
@@ -624,9 +785,9 @@
             small_first()
         if k > 2:
             small_next(k - 3)
-    for bit in range(max(fixed - 2, 0), bits_sp):
+    for bit in range(max(fixed - 2, 0), bits_sp if fixed else 0):
         small_next(bit)
-    if sp - 2 > fixed:
+    if sp - 2 > fixed and fixed:
 
         def both(k, _):
             ring_step(k, late)
@@ -651,7 +812,24 @@
             give_copy(g).start()
     ig_out[pl.ds(mine, half), :] = ig_sum[final]
     small_out[...] = small[bits_sp]
-    ring_end(early + late, (vg_out, gg_out, dg_out))
+    if paired:
+        for n in (2, 3, 0, 4, 1, 5):
+            settle(n, (vg_out, gg_out, dg_out))
+        for kind in range(2):
+            near_all(kind, 0).wait_send()
+            near_all(kind, 1).wait_send()
+        for at, ref in ((4, in_recv), (5, x_send), (6, z_send)):
+            send_to(at, ref, ref, near_recv.at[0], {"sp": flip(s, 0)}).wait_send()
+    else:
+        ring_end(early + late, (vg_out, gg_out, dg_out))
+        pltpu.make_async_remote_copy(
+            src_ref=ring_src,
+            dst_ref=ring_dst,
+            send_sem=ring_send.at[0],
+            recv_sem=ring_recv.at[0, 0],
+            device_id={"sp": ahead},
+            device_id_type=MESH,
+        ).wait_send()
 
     ig_copy(0, 0, ig_send, ig_recv, 0).wait_send()
     for bit in range(1, bits_dp):
@@ -666,14 +844,6 @@
         send_sem=small_ssem.at[0],
         recv_sem=small_rsem.at[0],
         device_id={"sp": flip(s, 0)},
-        device_id_type=MESH,
-    ).wait_send()
-    pltpu.make_async_remote_copy(
-        src_ref=ring_src,
-        dst_ref=ring_dst,
-        send_sem=ring_send.at[0],
-        recv_sem=ring_recv.at[0, 0],
-        device_id={"sp": ahead},
         device_id_type=MESH,
     ).wait_send()
 
@@ -732,7 +902,31 @@
     wide = is_wide(chunk, chans)
     lines, lanes = (chans, chunk) if wide else (chunk, chans)
     stat_rows = -(-2 * -(-tokens // 128) // 8) * 8
-    count = 3 * 2 * SUBS
+    paired = is_paired(sp, dp, chunk, chans)
+    if paired:
+        ring_shape, ring_sems, part_shape, turned_shape = (1, 1, 16, 128), (1, 1), (1, 8, 128), (1, 16, 128)
+    else:
+        count = 3 * 2 * SUBS
+        ring_shape, ring_sems = (count, sp - 1, lines // (2 * SUBS), lanes), (count, sp - 1)
+        part_shape, turned_shape = (3, sp * lines, lanes), (3, chans, tokens)
+    quads, hand = (sp // 4, chans // 2) if paired else (2, 16)
+    near, wide_chunk = (tokens, chunk) if paired else (16, 128)
+    pair_scratch = [
+        pltpu.VMEM((near, 2 * quads * wide_chunk), BF16),
+        pltpu.VMEM((near, 2 * quads * wide_chunk), BF16),
+        pltpu.VMEM((6, near, hand), BF16),
+        pltpu.VMEM((hand, 2 * near), BF16),
+        pltpu.VMEM((6, quads, hand, wide_chunk), BF16),
+        pltpu.VMEM((6, quads, hand, wide_chunk), BF16),
+        pltpu.VMEM((6, quads, hand, wide_chunk), F32),
+        pltpu.VMEM((6, quads - 1, hand, wide_chunk), BF16),
+        pltpu.VMEM((6, quads - 1, hand, wide_chunk), BF16),
+        pltpu.SemaphoreType.DMA((7,)),
+        pltpu.SemaphoreType.DMA((4,)),
+        pltpu.SemaphoreType.DMA((6,)),
+        pltpu.SemaphoreType.DMA((6,)),
+        pltpu.SemaphoreType.DMA((6, quads - 1)),
+    ]
     ig, vg, gg, dgrad, small = pl.pallas_call(
         functools.partial(kernel, sp, dp, ratio),
         out_shape=(
@@ -764,12 +958,12 @@
             pltpu.VMEM(extended, BF16),
             pltpu.VMEM(full, BF16),
             pltpu.VMEM(full, BF16),
-            pltpu.VMEM((3, chans, tokens), BF16),
+            pltpu.VMEM(turned_shape, BF16),
             pltpu.VMEM((2, tokens + 2 * PAD, 128), F32),
             pltpu.VMEM((4, dp, stat_rows, 128), F32),
-            pltpu.VMEM((3, sp * lines, lanes), F32),
-            pltpu.VMEM((count, sp - 1, lines // (2 * SUBS), lanes), BF16),
-            pltpu.VMEM((count, sp - 1, lines // (2 * SUBS), lanes), BF16),
+            pltpu.VMEM(part_shape, F32),
+            pltpu.VMEM(ring_shape, BF16),
+            pltpu.VMEM(ring_shape, BF16),
             pltpu.VMEM((half, width), BF16),
             pltpu.VMEM((half, width), BF16),
             pltpu.VMEM((half, width), F32),
@@ -782,12 +976,13 @@
             dma((4,)),
             dma((4,)),
             dma((1,)),
-            dma((count, sp - 1)),
+            dma(ring_sems),
             dma((bits_dp + 1,)),
             dma((bits_dp, GROUPS)),
             dma((1,)),
             dma((1,)),
             dma((bits_sp,)),
+            *pair_scratch,
         ],
         compiler_params=pltpu.CompilerParams(
             collective_id=0, has_side_effects=True, vmem_limit_bytes=MAIN

time: 53.3 us -> 50.7 us (0.951)
  Pallas kernels: 52.5 us -> 49.9 us
    pallas_call x1, Pallas kernels: 51.1 us -> 48.5 us  [on_device(): pl.pallas_call(functools.partial(kernel, sp, dp, ratio), out_shape=(pltpu...]
where the time goes in v3:
time: 50.7 us; the launch traced here: 50.6 us
  Pallas kernels  49.9 us (98%)
  between operations  0.64 us (1%)
    pallas_call x1, Pallas kernels, on_device(): pl.pallas_call(functools.partial(kernel, sp, dp, ratio), out_shape=(pltpu...  48.5 us
    pallas_call x1, Pallas kernels, on_device(): pl.pallas_call(functools.partial(finish, wide), out_shape=(jax.ShapeDtype...  1.4 us

profile of v3, /device:TPU:0, one launch (start us, length us, event | category | flops | bytes accessed | tf_op | source)
XLA Modules:
  0.0 50.6 jit_solution(2909242829404004694)
XLA Ops:
  0.6 48.5 %shard_map.152 = (bf16[320,2048]{1,0:T(8,128)(2,1)S(1)}, f32[256,256]{1,0:T(8,128)S(1)}, f32[256,256]{1,0:T(8,128)S(1)}, f32[256,256]{1,0:T(8,128)S(1)}, f32[40,256]{1,0:T(8,128)S(1)}) custom-call(bf16[320,2048]{1,0:T(8,128)(2,1)} %x_hbm.1, bf16[320,2048]{1,0:T(8,128)(2,1)} %og_hbm.1, bf16[2048,256]{1,0:T(8,128)(2,1)} %wv_hbm.1, bf16[2048,256]{1,0:T(8,128)(2,1)} %wg_hbm.1, ...), custom_call_target="tpu_custom_call" | custom-call | tf_op jit(solution)/shard_map/pallas_call | solution.py:930
  49.2 1.4 %shard_map.153 = (bf16[320,2048]{1,0:T(8,128)(2,1)}, f32[256,256]{1,0:T(8,128)}, f32[256,256]{1,0:T(8,128)}, f32[256,256]{1,0:T(8,128)}, f32[31,256]{1,0:T(8,128...) custom-call(bf16[320,2048]{1,0:T(8,128)(2,1)S(1)} %get-tuple-element.13.ig, f32[256,256]{1,0:T(8,128)S(1)} %get-tuple-element.14.vg, ...), custom_call_target="tpu_custom_call" | custom-call | tf_op jit(solution)/shard_map/pallas_call | solution.py:1002

commit v4 on v3

--- a/solution.py
+++ b/solution.py
@@ -19,6 +19,8 @@
 ROWS = 32
 SUBS = 2
 GROUPS = 2
+DIRECT = (0,)
+CUTS = 2
 MAIN = 61_900_000
 FINISH = 16_000_000
 
@@ -112,11 +114,14 @@
     held,
     z_send,
     z_recv,
+    z_send2,
+    z_recv2,
     pair_sends,
     near_recv,
     in_rsem,
     x_rsem,
     z_rsem,
+    cross_rsem,
 ):
     tokens, width = x.shape
     taps, chans = ck.shape
@@ -298,14 +303,10 @@
         return send_to(at, rows, rows, near_recv.at[at], where)
 
     halo_start(glu, 2 * PAD, 0)
-    near_start(0, slots[:1])
     for load in loads[3:]:
         load.wait()
-    near_start(1, slots[:1])
     d_act[own, :] = dot(og[...], wd[...], NT)
     halo_start(d_act, PAD, 2)
-    near_start(1, slots[1:])
-    near_start(0, slots[1:])
 
     span = ROWS + 2 * PAD
 
@@ -420,6 +421,8 @@
     row_loop(conv, begin=ROWS, end=ext - ROWS)
     moments_start(0)
     halo_wait(glu, 2 * PAD, 0)
+    near_start(1, slots)
+    near_start(0, slots)
 
     def conv_edge(i, _):
         conv(pl.multiple_of(i * (ext - ROWS), ROWS), None)
@@ -544,44 +547,73 @@
         where = {"sp": flip(s, in_bits[kind_of(n)])}
         return send_to(4, factor_of(n), in_recv.at[n], in_rsem.at[n], where)
 
-    def mid_copy(n):
+    strips = [pl.ds(cut * (hand // CUTS), hand // CUTS) for cut in range(CUTS)]
+
+    def mid_copy(n, cut):
         where = {"sp": flip(s, mid_bits[kind_of(n)])}
-        return send_to(5, x_send.at[n], x_recv.at[n], x_rsem.at[n], where)
-
-    def far_copy(n, far):
+        at, far = (7, 0) if n in DIRECT else (5, slice(None))
+        src, dst = x_send.at[n, far, strips[cut]], x_recv.at[n, far, strips[cut]]
+        return send_to(at, src, dst, x_rsem.at[n, cut], where)
+
+    def cross_copy(n, far):
+        at = DIRECT.index(n)
+        where = {"sp": flip(lax.rem(s + 4 * far, sp), mid_bits[kind_of(n)])}
+        return send_to(
+            8, z_send2.at[at, far - 1], z_recv2.at[at, far - 1], cross_rsem.at[at, far - 1], where
+        )
+
+    def far_copy(n, far, cut):
         where = {"sp": lax.rem(s + 4 * far, sp)}
-        return send_to(
-            6, z_send.at[n, far - 1], z_recv.at[n, far - 1], z_rsem.at[n, far - 1], where
-        )
+        src, dst = z_send.at[n, far - 1, strips[cut]], z_recv.at[n, far - 1, strips[cut]]
+        return send_to(6, src, dst, z_rsem.at[n, far - 1, cut], where)
+
+    def far_copies(n, far):
+        return [far_copy(n, far, cut) for cut in range(CUTS)]
 
     def product(n):
         kind = kind_of(n)
         in_copy(n).wait_recv()
         lhs[...] = jnp.concatenate([factor_of(n)[...], in_recv[n]], axis=0).T
-        for far, other in slots:
+        direct = n in DIRECT
+        for far, other in sorted(slots, key=lambda at: -at[0]) if direct else slots:
             mine = held_rows[kind][:, columns_of(s, far, other, kind)]
             rows = jnp.concatenate([mine, near_rows[kind][:, slot_of(far, other)]], axis=0)
             got = dot(lhs[...], rows, NN)
-            if other:
+            if direct and far:
+                sent = got.astype(BF16)
+                if other:
+                    z_send2[DIRECT.index(n), far - 1] = sent
+                else:
+                    z_send[n, far - 1] = sent
+                for copy in [cross_copy(n, far)] if other else far_copies(n, far):
+                    copy.start()
+            elif other:
                 x_send[n, far] = got.astype(BF16)
             else:
                 held[n, far] = got
-            if (far, other) == (quads - 1, 1):
-                mid_copy(n).start()
+            if (far, other) == (0 if direct else quads - 1, 1):
+                for cut in range(CUTS):
+                    mid_copy(n, cut).start()
 
     def meet(n):
-        mid_copy(n).wait_recv()
-        for far in range(1, quads):
-            z_send[n, far - 1] = (held[n, far] + x_recv[n, far].astype(F32)).astype(BF16)
-            far_copy(n, far).start()
-        held[n, 0] = held[n, 0] + x_recv[n, 0].astype(F32)
+        for cut, rows in enumerate(strips):
+            mid_copy(n, cut).wait_recv()
+            for far in () if n in DIRECT else range(1, quads):
+                got = held[n, far, rows, :] + x_recv[n, far, rows, :].astype(F32)
+                z_send[n, far - 1, rows, :] = got.astype(BF16)
+                far_copy(n, far, cut).start()
+            held[n, 0, rows, :] = held[n, 0, rows, :] + x_recv[n, 0, rows, :].astype(F32)
 
     def settle(n, outs):
         at, first = blocks[n]
         total = held[n, 0]
         for far in range(1, quads):
-            far_copy(n, far).wait_recv()
+            for copy in far_copies(n, far):
+                copy.wait_recv()
             total = total + z_recv[n, far - 1].astype(F32)
+            if n in DIRECT:
+                cross_copy(n, far).wait_recv()
+                total = total + z_recv2[DIRECT.index(n), far - 1].astype(F32)
         outs[at][pl.ds(first, hand), :] = ratio * total
 
     if paired:
@@ -601,13 +633,6 @@
 
     def norm_back(r, bias_sum):
         return bias_sum + down(back_rows(r, big))
-
-    second_wait(0)
-    bias_sum = row_loop(norm_back, zero, big, ROWS, ext - ROWS)
-    second_wait(1)
-    for (first, size), keep in zip(edges, kept):
-        bias_sum = bias_sum + down(back_rows(first, size)[keep])
-    halo_zero(d_pad, PAD)
 
     def conv_back(r, _):
         here = pl.ds(r, ROWS)
@@ -618,13 +643,22 @@
         dv[here, :] = grad.astype(BF16)
         dg[here, :] = (grad * value[here, :] * (1.0 - o)).astype(BF16)
 
-    middle = tokens // ROWS // 2 * ROWS
-    row_loop(conv_back, end=middle)
+    second_wait(0)
+    bias_sum = row_loop(norm_back, zero, big, ROWS, ext - ROWS)
+    row_loop(conv_back, begin=ROWS, end=tokens - ROWS)
+    second_wait(1)
+    for (first, size), keep in zip(edges, kept):
+        bias_sum = bias_sum + down(back_rows(first, size)[keep])
+    halo_zero(d_pad, PAD)
+
+    def back_edge(i, _):
+        conv_back(pl.multiple_of(i * (tokens - ROWS), ROWS), None)
+
+    lax.fori_loop(0, 2, back_edge, None)
     if not paired:
         ring_step(1, early)
-    row_loop(conv_back, begin=middle)
     if paired:
-        for n in (2, 3):
+        for n in range(2, 6):
             in_copy(n).start()
     else:
         grad_first(0, x, dv[...])
@@ -697,13 +731,22 @@
         for acc, tap in zip(sums, flat):
             small[0, tap : tap + 1, :] = jnp.sum(acc, axis=0, keepdims=True) * ratio
 
-    def small_copy(bit):
+    part_rows = small.shape[1] // 2
+    my_rows = pl.ds(pl.multiple_of(lax.rem(s, 2) * part_rows, 8), part_rows)
+
+    def small_copy(turn):
+        if turn == 0:
+            src, dst, bit = small.at[0], small_recv.at[0], 0
+        elif turn < bits_sp:
+            src, dst, bit = small.at[turn, my_rows], small_recv.at[turn, my_rows], turn
+        else:
+            src, dst, bit = small.at[turn, my_rows], small.at[turn, my_rows], 0
         return pltpu.make_async_remote_copy(
-            src_ref=small.at[bit],
-            dst_ref=small_recv.at[bit],
-            send_sem=small_ssem.at[0],
-            recv_sem=small_rsem.at[bit],
-            device_id={"sp": flip(s, (bit + 1) % bits_sp)},
+            src_ref=src,
+            dst_ref=dst,
+            send_sem=small_ssem.at[min(turn, 1)],
+            recv_sem=small_rsem.at[turn],
+            device_id={"sp": flip(s, bit)},
             device_id_type=MESH,
         )
 
@@ -713,12 +756,12 @@
         small[0, taps + 2 : taps + 3, :] = shift_sum * ratio
         small_copy(0).start()
 
-    def small_next(bit):
-        if bit < bits_sp:
-            small_copy(bit).wait_recv()
-            small[bit + 1] = small[bit] + small_recv[bit]
-            if bit + 1 < bits_sp:
-                small_copy(bit + 1).start()
+    def small_next(turn):
+        small_copy(turn).wait_recv()
+        if turn < bits_sp:
+            those = my_rows if turn else slice(None)
+            small[turn + 1, those, :] = small[turn, those, :] + small_recv[turn, those, :]
+            small_copy(turn + 1).start()
 
     def taps_half(lows):
         for low in lows:
@@ -749,8 +792,6 @@
             near_all(kind, 1).start()
         taps_half((0, 2, 4, 6))
         small_first()
-        for n in (4, 5):
-            in_copy(n).start()
     pair_sums()
     fixed = min(sp - 2, 6)
     if paired:
@@ -771,8 +812,8 @@
         meet(1)
         meet(5)
         small_next(2)
-        for bit in range(3, bits_sp):
-            small_next(bit)
+        for turn in range(3, bits_sp + 1):
+            small_next(turn)
         fixed = 0
     for k in range(1, fixed + 1):
         ring_step(k, late)
@@ -783,10 +824,10 @@
         if k == 2:
             taps_half((4, 6))
             small_first()
-        if k > 2:
+        if k > 2 and k - 3 <= bits_sp:
             small_next(k - 3)
-    for bit in range(max(fixed - 2, 0), bits_sp if fixed else 0):
-        small_next(bit)
+    for turn in range(max(fixed - 2, 0), bits_sp + 1 if fixed else 0):
+        small_next(turn)
     if sp - 2 > fixed and fixed:
 
         def both(k, _):
@@ -818,7 +859,10 @@
         for kind in range(2):
             near_all(kind, 0).wait_send()
             near_all(kind, 1).wait_send()
-        for at, ref in ((4, in_recv), (5, x_send), (6, z_send)):
+        waits = [(4, in_recv), (5, x_send.at[pl.ds(0, 6 - len(DIRECT))]), (6, z_send)]
+        if DIRECT:
+            waits += [(7, x_send.at[pl.ds(0, len(DIRECT)), 0]), (8, z_send2)]
+        for at, ref in waits:
             send_to(at, ref, ref, near_recv.at[0], {"sp": flip(s, 0)}).wait_send()
     else:
         ring_end(early + late, (vg_out, gg_out, dg_out))
@@ -837,15 +881,15 @@
     ig_copy(bits_dp, 0, ig_sum.at[final], ig_out.at[pl.ds(mine, half)], 0).wait()
     for at in range(4):
         stat_all(at).wait_send()
-    rounds = small.at[pl.ds(0, bits_sp)]
-    pltpu.make_async_remote_copy(
-        src_ref=rounds,
-        dst_ref=rounds,
-        send_sem=small_ssem.at[0],
-        recv_sem=small_rsem.at[0],
-        device_id={"sp": flip(s, 0)},
-        device_id_type=MESH,
-    ).wait_send()
+    for at, sent in ((0, small.at[0]), (1, small.at[pl.ds(1, bits_sp), my_rows])):
+        pltpu.make_async_remote_copy(
+            src_ref=sent,
+            dst_ref=sent,
+            send_sem=small_ssem.at[at],
+            recv_sem=small_rsem.at[0],
+            device_id={"sp": flip(s, 0)},
+            device_id_type=MESH,
+        ).wait_send()
 
 
 def finish(
@@ -893,7 +937,7 @@
     ratio = 1.0 / math.sqrt(tokens * sp)
     chunk = width // sp
     bits_sp, bits_dp = sp.bit_length() - 1, dp.bit_length() - 1
-    small_rows = -(-(taps + 3) // 8) * 8
+    small_rows = -(-(taps + 3) // 16) * 16
     half = tokens // 2
     full, extended = (tokens, chans), (tokens + 2 * PAD, chans)
     vmem = pl.BlockSpec(memory_space=pltpu.VMEM)
@@ -921,11 +965,14 @@
         pltpu.VMEM((6, quads, hand, wide_chunk), F32),
         pltpu.VMEM((6, quads - 1, hand, wide_chunk), BF16),
         pltpu.VMEM((6, quads - 1, hand, wide_chunk), BF16),
-        pltpu.SemaphoreType.DMA((7,)),
+        pltpu.VMEM((max(len(DIRECT), 1), quads - 1, hand, wide_chunk), BF16),
+        pltpu.VMEM((max(len(DIRECT), 1), quads - 1, hand, wide_chunk), BF16),
+        pltpu.SemaphoreType.DMA((9,)),
         pltpu.SemaphoreType.DMA((4,)),
         pltpu.SemaphoreType.DMA((6,)),
-        pltpu.SemaphoreType.DMA((6,)),
-        pltpu.SemaphoreType.DMA((6, quads - 1)),
+        pltpu.SemaphoreType.DMA((6, CUTS)),
+        pltpu.SemaphoreType.DMA((6, quads - 1, CUTS)),
+        pltpu.SemaphoreType.DMA((max(len(DIRECT), 1), quads - 1)),
     ]
     ig, vg, gg, dgrad, small = pl.pallas_call(
         functools.partial(kernel, sp, dp, ratio),
@@ -980,8 +1027,8 @@
             dma((bits_dp + 1,)),
             dma((bits_dp, GROUPS)),
             dma((1,)),
-            dma((1,)),
-            dma((bits_sp,)),
+            dma((2,)),
+            dma((bits_sp + 1,)),
             *pair_scratch,
         ],
         compiler_params=pltpu.CompilerParams(

time: 50.7 us -> 49.2 us (0.970)
  Pallas kernels: 49.9 us -> 48.4 us
    pallas_call x1, Pallas kernels: 48.5 us -> 47 us  [on_device(): pl.pallas_call(functools.partial(kernel, sp, dp, ratio), out_shape=(pltpu...]
where the time goes in v4:
time: 49.2 us; the launch traced here: 49 us
  Pallas kernels  48.4 us (98%)
  between operations  0.64 us (1%)
    pallas_call x1, Pallas kernels, on_device(): pl.pallas_call(functools.partial(kernel, sp, dp, ratio), out_shape=(pltpu...  47 us
    pallas_call x1, Pallas kernels, on_device(): pl.pallas_call(functools.partial(finish, wide), out_shape=(jax.ShapeDtype...  1.4 us

profile of v4, /device:TPU:0, one launch (start us, length us, event | category | flops | bytes accessed | tf_op | source)
XLA Modules:
  0.0 49.0 jit_solution(17664395332524255517)
XLA Ops:
  0.6 47.0 %shard_map.152 = (bf16[320,2048]{1,0:T(8,128)(2,1)S(1)}, f32[256,256]{1,0:T(8,128)S(1)}, f32[256,256]{1,0:T(8,128)S(1)}, f32[256,256]{1,0:T(8,128)S(1)}, f32[48,256]{1,0:T(8,128)S(1)}) custom-call(bf16[320,2048]{1,0:T(8,128)(2,1)} %x_hbm.1, bf16[320,2048]{1,0:T(8,128)(2,1)} %og_hbm.1, bf16[2048,256]{1,0:T(8,128)(2,1)} %wv_hbm.1, bf16[2048,256]{1,0:T(8,128)(2,1)} %wg_hbm.1, ...), custom_call_target="tpu_custom_call" | custom-call | tf_op jit(solution)/shard_map/pallas_call | solution.py:977
  47.6 1.4 %shard_map.153 = (bf16[320,2048]{1,0:T(8,128)(2,1)}, f32[256,256]{1,0:T(8,128)}, f32[256,256]{1,0:T(8,128)}, f32[256,256]{1,0:T(8,128)}, f32[31,256]{1,0:T(8,128...) custom-call(bf16[320,2048]{1,0:T(8,128)(2,1)S(1)} %get-tuple-element.13.ig, f32[256,256]{1,0:T(8,128)S(1)} %get-tuple-element.14.vg, ...), custom_call_target="tpu_custom_call" | custom-call | tf_op jit(solution)/shard_map/pallas_call | solution.py:1049

commit v5 on v4

--- a/solution.py
+++ b/solution.py
@@ -20,7 +20,7 @@
 SUBS = 2
 GROUPS = 2
 DIRECT = (0,)
-CUTS = 2
+CUTS = 1
 MAIN = 61_900_000
 FINISH = 16_000_000
 
@@ -167,7 +167,7 @@
             ]
         )
     ]
-    for load in loads:
+    for load in loads[:3]:
         load.start()
 
     barrier = pltpu.get_barrier_semaphore()
@@ -183,7 +183,10 @@
             barrier, inc=1, device_id={"dp": lax.rem(d + off, dp)}, device_id_type=MESH
         )
 
-    for load in loads[:3]:
+    loads[0].wait()
+    for load in loads[3:]:
+        load.start()
+    for load in loads[1:3]:
         load.wait()
     value_f, gate_f = dot(x[...], wv[...], NN), dot(x[...], wg[...], NN)
     value[...] = value_f.astype(BF16).astype(F32)
@@ -804,8 +807,8 @@
         product(1)
         product(4)
         product(5)
+        small_next(1)
         meet(2)
-        small_next(1)
         meet(3)
         meet(0)
         meet(4)

time: 49.2 us -> 49.2 us (level)
  no operation moved by 1% of the time
where the time goes in v5:
time: 49.2 us; the launch traced here: 49 us
  Pallas kernels  48.4 us (98%)
  between operations  0.64 us (1%)
    pallas_call x1, Pallas kernels, on_device(): pl.pallas_call(functools.partial(kernel, sp, dp, ratio), out_shape=(pltpu...  47 us
    pallas_call x1, Pallas kernels, on_device(): pl.pallas_call(functools.partial(finish, wide), out_shape=(jax.ShapeDtype...  1.4 us

profile of v5, /device:TPU:0, one launch (start us, length us, event | category | flops | bytes accessed | tf_op | source)
XLA Modules:
  0.0 49.0 jit_solution(7820441946878171874)
XLA Ops:
  0.6 47.0 %shard_map.152 = (bf16[320,2048]{1,0:T(8,128)(2,1)S(1)}, f32[256,256]{1,0:T(8,128)S(1)}, f32[256,256]{1,0:T(8,128)S(1)}, f32[256,256]{1,0:T(8,128)S(1)}, f32[48,256]{1,0:T(8,128)S(1)}) custom-call(bf16[320,2048]{1,0:T(8,128)(2,1)} %x_hbm.1, bf16[320,2048]{1,0:T(8,128)(2,1)} %og_hbm.1, bf16[2048,256]{1,0:T(8,128)(2,1)} %wv_hbm.1, bf16[2048,256]{1,0:T(8,128)(2,1)} %wg_hbm.1, ...), custom_call_target="tpu_custom_call" | custom-call | tf_op jit(solution)/shard_map/pallas_call | solution.py:980
  47.6 1.4 %shard_map.153 = (bf16[320,2048]{1,0:T(8,128)(2,1)}, f32[256,256]{1,0:T(8,128)}, f32[256,256]{1,0:T(8,128)}, f32[256,256]{1,0:T(8,128)}, f32[31,256]{1,0:T(8,128...) custom-call(bf16[320,2048]{1,0:T(8,128)(2,1)S(1)} %get-tuple-element.13.ig, f32[256,256]{1,0:T(8,128)S(1)} %get-tuple-element.14.vg, ...), custom_call_target="tpu_custom_call" | custom-call | tf_op jit(solution)/shard_map/pallas_call | solution.py:1052
